TPU v7x, 256 devices: a whole 4x4x8 slice. The times are simulated.
256 devices in a mesh: sp: 32 (over z, y), tp: 8 (over x, core).
Axes of the slice: x: 4, y: 4, z: 8, core: 2. Of those that a mesh axis runs over, the one named last changes fastest.
Arguments:
- inputs: bfloat16 [2, 12288, 4096], P(None, 'sp'), may hold values from -8 to 8
- w_key: bfloat16 [4096, 2048], P(None, 'tp'), may hold values from -0.09375 to 0.09375
- w_value: bfloat16 [4096, 2048], P(None, 'tp'), may hold values from -0.09375 to 0.09375
- w_query: bfloat16 [4096, 2048], P(None, 'tp'), may hold values from -0.09375 to 0.09375
- w_igate: bfloat16 [4096, 16], replicated, may hold values from -1 to 1
- w_fgate: bfloat16 [4096, 16], replicated, may hold values from -0.09375 to 0.09375
- forget_bias: float32 [16], replicated, may hold values from 3 to 12
- new_rows: bfloat16 [2, 4096], P(None, 'tp'), may hold values from -6 to 6
Outputs:
- cache_matrix: bfloat16 [2, 16, 128, 128], P(None, 'tp', 'sp')
- cache_normal: float32 [2, 16, 128], P(None, 'tp', 'sp')
- cache_top: float32 [2, 16], P(None, 'tp')
- read: bfloat16 [2, 16, 128], P(None, 'tp', 'sp')
All inputs are finite; a program needn't handle non-finite values.
Results may differ from a plain program's by a relative error of at most 0.015.
Values may be sent and summed in bfloat16 or wider, within the bound.
A program may use at most 64 MiB of HBM per device.

v0:
```python
import jax
import jax.numpy as jnp
from jax import lax
from jax.sharding import PartitionSpec as P

DH = 128


EPS = 1e-06


def from_everyone(value, axis):
    copies = jnp.broadcast_to(value, (lax.axis_size(axis), *value.shape))
    return lax.all_to_all(copies, axis, split_axis=0, concat_axis=0, tiled=True)


def combined_pairwise(pieces, combine):
    while len(jax.tree.leaves(pieces)[0]) > 1:
        pieces = jax.vmap(combine)(*(pieces[side::2] for side in (0, 1)))
    return pieces[0]


def entering(value, axis, combine, identity):
    devices, here = (lax.axis_size(axis), lax.axis_index(axis))
    passed = jnp.arange(devices) > here

    def kept(part, zero, own):
        part = jnp.where(
            passed.reshape(-1, *(1 for _ in own.shape)), part, jnp.asarray(zero, own.dtype)
        )
        return part[::-1]

    pieces = from_everyone(value, axis)
    return combined_pairwise(kept(pieces, identity, value), combine)


def of_everyone(value, axis):
    return from_everyone(value, axis).max(axis=0)


def split_up(value, dim, devices):
    before, after = (value.shape[:dim], value.shape[dim + 1 :])
    return jnp.moveaxis(value.reshape(*before, devices, -1, *after), dim, 0)


def summed_on_arrival(value, axis, dim):
    tiles = split_up(value, dim, lax.axis_size(axis))
    arrived = lax.all_to_all(tiles, axis, split_axis=0, concat_axis=0, tiled=True)
    return arrived.sum(axis=0)


def in_order(tiles, dim):
    shape = list(tiles.shape[1:])
    shape[dim] *= tiles.shape[0]
    return jnp.moveaxis(tiles, 0, dim).reshape(shape)


def collect(value, axis, dim):
    tiles = from_everyone(value, axis)
    return in_order(tiles, dim)


def over_copies(value, axis):
    everything = from_everyone(value, axis)
    return jnp.sum(everything, axis=0)


def normalize(row_block):
    scaled = row_block.astype(jnp.float32)
    scaled = scaled * lax.rsqrt(jnp.mean(scaled * scaled, axis=-1, keepdims=True) + EPS)
    return scaled.astype(jnp.bfloat16)


def add_pair(earlier, second):
    return earlier + second


def shards(inputs, w_key, w_value, w_query, w_igate, w_fgate, forget_bias, new_rows):
    head_count = w_key.shape[1] // DH
    seq_count, span, width = inputs.shape
    rows_own = DH // lax.axis_size("sp")
    row_start = lax.axis_index("sp") * rows_own
    head_start = lax.axis_index("tp") * head_count
    gate_in = lax.dynamic_slice_in_dim(w_igate, head_start, head_count, 1)
    gate_forget = lax.dynamic_slice_in_dim(w_fgate, head_start, head_count, 1)
    bias_heads = lax.dynamic_slice_in_dim(forget_bias, head_start, head_count, 0)
    normed = normalize(inputs)
    key_rows = jnp.einsum("spd,dc->spc", normed, w_key, preferred_element_type=jnp.float32).astype(
        jnp.bfloat16
    )
    value_rows = jnp.einsum(
        "spd,dc->spc", normed, w_value, preferred_element_type=jnp.float32
    ).astype(jnp.bfloat16)
    input_pre = jnp.einsum("spd,dh->sph", normed, gate_in, preferred_element_type=jnp.float32)
    log_forget = jax.nn.log_sigmoid(
        jnp.einsum("spd,dh->sph", normed, gate_forget, preferred_element_type=jnp.float32)
        + bias_heads
    )
    running = jnp.cumsum(log_forget, axis=1)
    own_total = running[:, -1, :]
    beyond = entering(own_total, "sp", add_pair, jnp.zeros_like(own_total))
    log_weight = (beyond + own_total)[:, None, :] - running + input_pre
    stabilizer = of_everyone(jnp.max(log_weight, axis=1), "sp")
    weight = jnp.exp(log_weight - stabilizer[:, None, :])
    key_heads = key_rows.reshape(seq_count, span, head_count, DH)
    value_heads = value_rows.reshape(seq_count, span, head_count, DH)
    weighted = (weight[..., None] * value_heads.astype(jnp.float32)).astype(jnp.bfloat16)
    partial_normal = jnp.einsum("sth,sthd->shd", weight, key_heads.astype(jnp.float32))
    partial_matrix = jnp.einsum(
        "sthe,sthd->shed", weighted, key_heads, preferred_element_type=jnp.float32
    )
    matrix, normal = (
        summed_on_arrival(partial_matrix, "sp", 2),
        summed_on_arrival(partial_normal, "sp", 2),
    )
    cache_matrix = matrix.astype(jnp.bfloat16)
    new_normed = normalize(collect(new_rows, "tp", 1))
    query_new = jnp.dot(new_normed, w_query, preferred_element_type=jnp.float32).astype(
        jnp.bfloat16
    )
    key_new = jnp.dot(new_normed, w_key, preferred_element_type=jnp.float32).astype(jnp.bfloat16)
    value_new = jnp.dot(new_normed, w_value, preferred_element_type=jnp.float32).astype(
        jnp.bfloat16
    )
    query_new = query_new.astype(jnp.float32).reshape(seq_count, head_count, DH)
    key_new = key_new.astype(jnp.float32).reshape(seq_count, head_count, DH)
    value_new = value_new.astype(jnp.float32).reshape(seq_count, head_count, DH)
    value_own = lax.dynamic_slice_in_dim(value_new, row_start, rows_own, 2)
    query_own = lax.dynamic_slice_in_dim(query_new, row_start, rows_own, 2)
    input_new = jnp.dot(new_normed, gate_in, preferred_element_type=jnp.float32)
    forget_new = jax.nn.log_sigmoid(
        jnp.dot(new_normed, gate_forget, preferred_element_type=jnp.float32) + bias_heads
    )
    top_next = jnp.maximum(forget_new + stabilizer, input_new)
    old_share = jnp.exp(forget_new + stabilizer - top_next)
    new_share = jnp.exp(input_new - top_next)
    agreement = jnp.sum(key_new * query_new, axis=-1)
    factor = DH ** (-0.5)
    numerator = old_share[..., None] * jnp.einsum(
        "shed,shd->she", cache_matrix.astype(jnp.float32), query_new
    )
    numerator = (numerator + (new_share * agreement)[..., None] * value_own) * factor
    normal_dot = over_copies(jnp.sum(normal * query_own, axis=-1), "sp")
    denominator = (old_share * normal_dot + new_share * agreement) * factor
    read = numerator / jnp.maximum(jnp.abs(denominator), 1.0)[..., None]
    return (cache_matrix, normal, stabilizer, read.astype(jnp.bfloat16))


def solution(mesh):
    in_specs = (
        P(None, "sp", None),
        P(None, "tp"),
        P(None, "tp"),
        P(None, "tp"),
        P(),
        P(),
        P(),
        P(None, "tp"),
    )
    out_specs = (P(None, "tp", "sp", None), P(None, "tp", "sp"), P(None, "tp"), P(None, "tp", "sp"))
    return jax.shard_map(shards, mesh=mesh, in_specs=in_specs, out_specs=out_specs, check_vma=False)
```

profile of v0, /device:TPU:1, one launch (start us, length us, event | category | flops | bytes accessed | tf_op | source)
XLA Modules:
  0.0 112.7 jit_solution(5783288280995298979)
XLA Ops:
  0.7 4.2 %fusion = f32[2,384]{1,0:T(2,128)S(1)} fusion(bf16[2,384,4096]{2,1,0:T(8,128)(2,1)} %param.8), kind=kLoop, calls=%fused_computation.2 | loop fusion | flops 9436416 | bytes 6294528 | tf_op jit(solution)/shard_map/reduce_sum | solution.py:70
  4.9 0.1 dynamic_slice.16
  5.0 4.6 %fusion.49 = f32[2,2,384]{2,1,0:T(2,128)S(1)} fusion(bf16[4096,16]{0,1:T(8,128)(2,1)} %param.13, s32[]{:T(128)S(6)} %select_n.24, bf16[2,384,4096]{2,1,0:T(8,128)(2,1)} %param.8, f32[2,384]{1,0:T(2,128)S(1)} %add_rsqrt_fusion, f32[2]{0:T(128)S(1)} %dynamic_slice.16), kind=kOutput, calls=%fused_computation.44 | convolution fusion | flops 22033920 | bytes 6317068 | tf_op jit(solution)/shard_map/spd,dh->sph/dot_general | solution.py:96
  9.6 1.2 %reduce-window.6 = f32[2,2,3,128]{3,2,1,0:T(4,128)S(1)} reduce-window(f32[2,2,3,128]{3,2,1,0:T(4,128)S(1)} %reshape.80, f32[]{:T(128)} %constant.16.clone.1), window={size=1x1x1x128 pad=0_0x0_0x0_0x127_0}, to_apply=%region_1.2 | reduce-window | flops 195072 | bytes 12292 | tf_op jit(solution)/shard_map/reduce-window
  10.9 0.2 slice_reduce_fusion
  11.0 0.3 reduce-window.9
  11.4 0.1 broadcast_add_fusion
  11.5 0.2 slice_reduce_fusion.1
  11.6 0.6 broadcast_in_dim.21
  12.2 12.0 %all-to-all-start = ((f32[32,2,2]{2,1,0:T(2,128)}), f32[32,2,2]{2,1,0:T(2,128)S(1)}, u32[]{:S(2)}, u32[]{:S(2)}) async-start(f32[32,2,2]{2,1,0:T(2,128)} %broadcast_in_dim.21), calls=%async_computation | async-start | bytes 65536 | tf_op jit(solution)/shard_map/all_to_all | solution.py:14
  24.3 5.4 %fusion.17 = bf16[2,384,256]{1,2,0:T(8,128)(2,1)S(1)} fusion(bf16[4096,256]{1,0:T(8,128)(2,1)} %param.9, bf16[2,384,4096]{2,1,0:T(8,128)(2,1)} %param.8, f32[2,384]{1,0:T(2,128)S(1)} %add_rsqrt_fusion), kind=kOutput, calls=%fused_computation.11 | convolution fusion | flops 1620246528 | bytes 8784896 | tf_op jit(solution)/shard_map/spd,dc->spc/dot_general | solution.py:88
  29.7 3.3 %all-to-all-done = f32[32,2,2]{2,1,0:T(2,128)S(1)} async-done(((f32[32,2,2]{2,1,0:T(2,128)}), f32[32,2,2]{2,1,0:T(2,128)S(1)}, u32[]{:S(2)}, u32[]{:S(2)}) %all-to-all-start) | async-done | bytes 544 | tf_op jit(solution)/shard_map/all_to_all | solution.py:14
  33.0 0.1 broadcast_select_fusion
  33.2 0.1 copy.41
  33.3 0.2 add_reduce_fusion
  33.4 4.7 %fusion.72 = (f32[2,2]{1,0:T(2,128)S(1)}, f32[2,384,2]{1,2,0:T(2,128)S(1)}) fusion(bf16[4096,16]{0,1:T(8,128)(2,1)} %param.12, s32[]{:T(128)S(6)} %select_n.24, bf16[2,384,4096]{2,1,0:T(8,128)(2,1)} %param.8, f32[2,384]{1,0:T(2,128)S(1)} %add_rsqrt_fusion, f32[2,2,384]{2,1,0:T(2,128)S(1)} %reduce_window_sum.16, f32[2,2]{1,0:T(2,128)S(1)} %add_reduce_fusion), kind=kOutput, calls=%fused_computation.76 | convolution fusion | flops 22024700 | bytes 6323236 | tf_op jit(solution)/shard_map/spd,dh->sph/dot_general | solution.py:94
  38.1 0.6 broadcast_in_dim.37
  38.7 6.0 %all-to-all-start.1 = ((f32[32,2,2]{2,1,0:T(2,128)}), f32[32,2,2]{2,1,0:T(2,128)S(1)}, u32[]{:S(2)}, u32[]{:S(2)}) async-start(f32[32,2,2]{2,1,0:T(2,128)} %broadcast_in_dim.37), calls=%async_computation.1 | async-start | bytes 65536 | tf_op jit(solution)/shard_map/all_to_all | solution.py:14
  44.7 4.8 %fusion.12 = bf16[2,384,256]{1,2,0:T(8,128)(2,1)S(1)} fusion(bf16[4096,256]{1,0:T(8,128)(2,1)S(1)} %copy-done, bf16[2,384,4096]{2,1,0:T(8,128)(2,1)} %param.8, f32[2,384]{1,0:T(2,128)S(1)} %add_rsqrt_fusion), kind=kOutput, calls=%fused_computation.10 | convolution fusion | flops 1620246528 | bytes 8784896 | tf_op jit(solution)/shard_map/spd,dc->spc/dot_general | solution.py:91
  49.5 3.9 %all-to-all-done.1 = f32[32,2,2]{2,1,0:T(2,128)S(1)} async-done(((f32[32,2,2]{2,1,0:T(2,128)}), f32[32,2,2]{2,1,0:T(2,128)S(1)}, u32[]{:S(2)}, u32[]{:S(2)}) %all-to-all-start.1) | async-done | bytes 544 | tf_op jit(solution)/shard_map/all_to_all | solution.py:14
  53.4 0.1 fusion.86
  53.5 0.2 fusion.50
  53.7 0.1 reshape.84
  53.9 0.7 copy.47
  54.5 5.3 %all-to-all-start.3 = ((f32[32,2,2,4]{3,2,1,0:T(2,128)}), f32[32,2,2,4]{3,2,1,0:T(2,128)S(1)}, u32[]{:S(2)}, u32[]{:S(2)}) async-start(f32[32,2,2,4]{3,2,1,0:T(2,128)} %copy.47), calls=%async_computation.3 | async-start | bytes 131072 | tf_op jit(solution)/shard_map/all_to_all | solution.py:48
  59.9 0.1 subtract_exponential_fusion
  59.9 8.7 %all-to-all-done.3 = f32[32,2,2,4]{3,2,1,0:T(2,128)S(1)} async-done(((f32[32,2,2,4]{3,2,1,0:T(2,128)}), f32[32,2,2,4]{3,2,1,0:T(2,128)S(1)}, u32[]{:S(2)}, u32[]{:S(2)}) %all-to-all-start.3) | async-done | bytes 2080 | tf_op jit(solution)/shard_map/all_to_all | solution.py:48
  68.7 0.6 broadcast_in_dim.38
  69.3 7.5 %all-to-all-start.4 = ((bf16[8,2,512]{2,1,0:T(2,128)(2,1)}), bf16[8,2,512]{2,1,0:T(2,128)(2,1)S(1)}, u32[]{:S(2)}, u32[]{:S(2)}) async-start(bf16[8,2,512]{2,1,0:T(2,128)(2,1)} %broadcast_in_dim.38), calls=%async_computation.4 | async-start | bytes 32768 | tf_op jit(solution)/shard_map/all_to_all | solution.py:14
  76.8 0.3 fusion.38
  77.1 0.7 copy.67
  77.9 3.6 %all-to-all-done.4 = bf16[8,2,512]{2,1,0:T(2,128)(2,1)S(1)} async-done(((bf16[8,2,512]{2,1,0:T(2,128)(2,1)}), bf16[8,2,512]{2,1,0:T(2,128)(2,1)S(1)}, u32[]{:S(2)}, u32[]{:S(2)}) %all-to-all-start.4) | async-done | bytes 16416 | tf_op jit(solution)/shard_map/all_to_all | solution.py:14
  81.5 0.1 fusion.41
  81.6 0.1 multiply_convert_fusion
  81.7 0.4 fusion.35
  82.1 2.0 %convolution_convert_fusion.2 = bf16[2,256]{1,0:T(2,128)(2,1)S(1)} fusion(bf16[2,4096]{1,0:T(2,128)(2,1)S(1)} %multiply_convert_fusion, bf16[4096,256]{1,0:T(8,128)(2,1)} %param.11), kind=kOutput, calls=%fused_computation.18 | convolution fusion | flops 4194816 | bytes 2114560 | tf_op jit(solution)/shard_map/dot_general | solution.py:118
  84.1 0.2 multiply_reduce_fusion
  84.3 0.6 broadcast_in_dim.39
  84.9 3.8 %all-to-all-start.5 = ((f32[32,2,2]{2,1,0:T(2,128)}), f32[32,2,2]{2,1,0:T(2,128)S(1)}, u32[]{:S(2)}, u32[]{:S(2)}) async-start(f32[32,2,2]{2,1,0:T(2,128)} %broadcast_in_dim.39), calls=%async_computation.5 | async-start | bytes 65536 | tf_op jit(solution)/shard_map/all_to_all | solution.py:14
  88.7 2.0 %fusion.34 = f32[2,256]{1,0:T(2,128)S(1)} fusion(bf16[2,4096]{1,0:T(2,128)(2,1)S(1)} %multiply_convert_fusion, bf16[4096,256]{1,0:T(8,128)(2,1)} %param.9), kind=kOutput, calls=%fused_computation.19 | convolution fusion | flops 4195328 | bytes 2115584 | tf_op jit(solution)/shard_map/dot_general | solution.py:121
  90.8 6.6 %all-to-all-done.5 = f32[32,2,2]{2,1,0:T(2,128)S(1)} async-done(((f32[32,2,2]{2,1,0:T(2,128)}), f32[32,2,2]{2,1,0:T(2,128)S(1)}, u32[]{:S(2)}, u32[]{:S(2)}) %all-to-all-start.5) | async-done | bytes 544 | tf_op jit(solution)/shard_map/all_to_all | solution.py:14
  97.4 3.9 %all-to-all-start.2 = ((f32[32,2,2,4,128]{4,3,2,1,0:T(4,128)}), f32[32,2,2,4,128]{4,3,2,1,0:T(4,128)S(1)}, u32[]{:S(2)}, u32[]{:S(2)}) async-start(f32[32,2,2,4,128]{4,3,2,1,0:T(4,128)} %bitcast.57), calls=%async_computation.2 | async-start | bytes 524288 | tf_op jit(solution)/shard_map/all_to_all | solution.py:48
  101.2 0.1 multiply_reduce_fusion.1
  101.3 1.0 fusion.44
  102.4 1.0 abs_maximum_fusion
  103.4 8.4 %all-to-all-done.2 = f32[32,2,2,4,128]{4,3,2,1,0:T(4,128)S(1)} async-done(((f32[32,2,2,4,128]{4,3,2,1,0:T(4,128)}), f32[32,2,2,4,128]{4,3,2,1,0:T(4,128)S(1)}, u32[]{:S(2)}, u32[]{:S(2)}) %all-to-all-start.2) | async-done | bytes 262176 | tf_op jit(solution)/shard_map/all_to_all | solution.py:48
  111.9 0.1 fusion.73
  112.0 0.6 fusion.56
  (34 shorter events, 0.4 us)
Async XLA Ops:
  0.6 44.0 %copy-start = (bf16[4096,256]{1,0:T(8,128)(2,1)S(1)}, bf16[4096,256]{1,0:T(8,128)(2,1)}, u32[]{:S(2)}) copy-start(bf16[4096,256]{1,0:T(8,128)(2,1)} %param.10) | copy-start | bytes 6291460
  0.6 4.3 %copy-start.5 = (f32[16]{0:T(128)S(1)}, f32[16]{0:T(128)}, u32[]{:S(2)}) copy-start(f32[16]{0:T(128)} %param.14) | copy-start | bytes 196
  12.2 20.7 %all-to-all-start = ((f32[32,2,2]{2,1,0:T(2,128)}), f32[32,2,2]{2,1,0:T(2,128)S(1)}, u32[]{:S(2)}, u32[]{:S(2)}) async-start(f32[32,2,2]{2,1,0:T(2,128)} %broadcast_in_dim.21), calls=%async_computation | async-start | bytes 65536 | tf_op jit(solution)/shard_map/all_to_all | solution.py:14
  38.7 14.7 %all-to-all-start.1 = ((f32[32,2,2]{2,1,0:T(2,128)}), f32[32,2,2]{2,1,0:T(2,128)S(1)}, u32[]{:S(2)}, u32[]{:S(2)}) async-start(f32[32,2,2]{2,1,0:T(2,128)} %broadcast_in_dim.37), calls=%async_computation.1 | async-start | bytes 65536 | tf_op jit(solution)/shard_map/all_to_all | solution.py:14
  44.7 24.0 %copy-start.4 = (bf16[2,512]{1,0:T(2,128)(2,1)S(1)}, bf16[2,512]{1,0:T(2,128)(2,1)}, u32[]{:S(2)}) copy-start(bf16[2,512]{1,0:T(2,128)(2,1)} %param.15) | copy-start | bytes 6148
  53.4 59.2 %copy-start.1 = (f32[2,2]{1,0:T(2,128)}, f32[2,2]{1,0:T(2,128)S(1)}, u32[]{:S(2)}) copy-start(f32[2,2]{1,0:T(2,128)S(1)} %reduce_max.19) | copy-start | bytes 52
  54.5 14.1 %all-to-all-start.3 = ((f32[32,2,2,4]{3,2,1,0:T(2,128)}), f32[32,2,2,4]{3,2,1,0:T(2,128)S(1)}, u32[]{:S(2)}, u32[]{:S(2)}) async-start(f32[32,2,2,4]{3,2,1,0:T(2,128)} %copy.47), calls=%async_computation.3 | async-start | bytes 131072 | tf_op jit(solution)/shard_map/all_to_all | solution.py:48
  69.3 12.2 %all-to-all-start.4 = ((bf16[8,2,512]{2,1,0:T(2,128)(2,1)}), bf16[8,2,512]{2,1,0:T(2,128)(2,1)S(1)}, u32[]{:S(2)}, u32[]{:S(2)}) async-start(bf16[8,2,512]{2,1,0:T(2,128)(2,1)} %broadcast_in_dim.38), calls=%async_computation.4 | async-start | bytes 32768 | tf_op jit(solution)/shard_map/all_to_all | solution.py:14
  77.9 34.7 %copy-start.2 = (f32[2,2,4]{2,1,0:T(2,128)}, f32[2,2,4]{2,1,0:T(2,128)S(1)}, u32[]{:S(2)}) copy-start(f32[2,2,4]{2,1,0:T(2,128)S(1)} %reduce_sum.65) | copy-start | bytes 196
  84.9 12.5 %all-to-all-start.5 = ((f32[32,2,2]{2,1,0:T(2,128)}), f32[32,2,2]{2,1,0:T(2,128)S(1)}, u32[]{:S(2)}, u32[]{:S(2)}) async-start(f32[32,2,2]{2,1,0:T(2,128)} %broadcast_in_dim.39), calls=%async_computation.5 | async-start | bytes 65536 | tf_op jit(solution)/shard_map/all_to_all | solution.py:14
  97.4 14.5 %all-to-all-start.2 = ((f32[32,2,2,4,128]{4,3,2,1,0:T(4,128)}), f32[32,2,2,4,128]{4,3,2,1,0:T(4,128)S(1)}, u32[]{:S(2)}, u32[]{:S(2)}) async-start(f32[32,2,2,4,128]{4,3,2,1,0:T(4,128)} %bitcast.57), calls=%async_computation.2 | async-start | bytes 524288 | tf_op jit(solution)/shard_map/all_to_all | solution.py:48
  111.9 0.8 copy-start.3
where the time goes:
time: 114 us; the launch traced here: 113 us
  starting transfers between devices  38.5 us (34%)
  waiting for transfers between devices  34.5 us (30%)
  matrix products  26.4 us (23%)
  other arithmetic  7.66 us (7%)
  local copies, waits for them, and re-layouts  4.67 us (4%)
    all_to_all x4, starting transfers between devices, from_everyone(): return lax.all_to_all(copies, axis, split_axis=0, concat_axis=0, tiled=True)  29.3 us
    all_to_all x4, waiting for transfers between devices, from_everyone(): return lax.all_to_all(copies, axis, split_axis=0, concat_axis=0, tiled=True)  17.4 us
    all_to_all x2, waiting for transfers between devices, summed_on_arrival(): lax.all_to_all(tiles, axis, split_axis=0, concat_axis=0, tiled=True)  17.2 us
    all_to_all x2, starting transfers between devices, summed_on_arrival(): lax.all_to_all(tiles, axis, split_axis=0, concat_axis=0, tiled=True)  9.18 us
    dot_general x1, matrix products, shards(): jnp.einsum('spd,dc->spc', normed, w_key, preferred_element_type=jnp.float32)  5.4 us
    dot_general x1, matrix products, shards(): jnp.einsum('spd,dc->spc', normed, w_value, preferred_element_type=jnp.flo...  4.77 us
    dot_general x1, matrix products, shards(): jnp.einsum('spd,dh->sph', normed, gate_in, preferred_element_type=jnp.flo...  4.66 us
    dot_general x1, matrix products, shards(): jnp.einsum('spd,dh->sph', normed, gate_forget, preferred_element_type=jnp...  4.61 us
  transfers between devices with their start and end apart: 6, of which 6 were waited for; matrix products, arithmetic and copies ran while one was open for 14% of the time, Pallas kernels for 0%

commit v1 on v0

v1 whole, which is shorter than its diff:
```python
import functools

import jax
import jax.numpy as jnp
from jax import lax
from jax.experimental import pallas as pl
from jax.experimental.pallas import tpu as pltpu
from jax.sharding import PartitionSpec as P

DH = 128
EPS = 1e-06
MESH = pl.DeviceIdType.MESH
F32 = jnp.float32
BF16 = jnp.bfloat16
NZ, NY = 8, 4
SP, TP = NZ * NY, 8
CHUNKS = 2
BLOCKS = ((0, 128), (128, 256), (384, 384))
MSG = 24


def peer_offsets():
    offsets = [(dz, dy) for dz in range(NZ) for dy in range(NY) if dz or dy]
    return sorted(offsets, key=lambda o: -(min(o[0], NZ - o[0]) + min(o[1], NY - o[1])))


def iota(shape, dim):
    return lax.broadcasted_iota(jnp.int32, shape, dim)


def log_sigmoid(v):
    u = jnp.exp(-jnp.abs(v))
    series = u * (1.0 - u * (0.5 - u * (1.0 / 3.0 - u * (0.25 - u * (0.2 - u * (1.0 / 6.0))))))
    return jnp.minimum(v, 0.0) - jnp.where(u < 0.03, series, jnp.log(1.0 + u))


def split3(v):
    hi = v.astype(BF16).astype(F32)
    rest = v - hi
    mid = rest.astype(BF16).astype(F32)
    return hi, mid, rest - mid


def kernel(
    x_hbm, wk_hbm, wv_hbm, wq_hbm, wi_hbm, wf_hbm, bias_hbm, new_hbm,
    mat_out, nrm_out, top_out, read_out,
    x, xn, wk, wv, wq, wg, bias, fresh, keys, values, acc_g, tri, wrow, stat,
    send_m, recv_m, send_s, recv_s,
    load_sem, x_sem, w_sem, new_sem, msem, ssem,
):
    sp, tp = lax.axis_index("sp"), lax.axis_index("tp")
    z, y = sp // NY, lax.rem(sp, NY)
    rows, width = x.shape
    span = rows // 2
    step = width // CHUNKS
    peers = []
    for dz, dy in peer_offsets():
        peers.append(lax.rem(z + dz, NZ) * NY + lax.rem(y + dy, NY))
    tp_peers = [lax.rem(tp + k, TP) for k in range(1, TP)]

    small = [
        pltpu.make_async_copy(wi_hbm, wg.at[pl.ds(0, 16)], load_sem.at[0]),
        pltpu.make_async_copy(wf_hbm, wg.at[pl.ds(16, 16)], load_sem.at[1]),
        pltpu.make_async_copy(bias_hbm, bias, load_sem.at[2]),
        pltpu.make_async_copy(new_hbm, fresh.at[tp], load_sem.at[3]),
    ]
    x_loads = []
    for i, (at, count) in enumerate(BLOCKS):
        part = pl.ds(at, count)
        x_loads.append(pltpu.make_async_copy(x_hbm.at[part], x.at[part], x_sem.at[i]))
    w_loads = []
    for c in range(CHUNKS):
        part = pl.ds(c * step, step)
        w_loads.append(pltpu.make_async_copy(wv_hbm.at[part], wv.at[part], w_sem.at[c, 0]))
        w_loads.append(pltpu.make_async_copy(wk_hbm.at[part], wk.at[part], w_sem.at[c, 1]))
    load_q = pltpu.make_async_copy(wq_hbm, wq, load_sem.at[4])
    for copy in (x_loads[0], *small, *w_loads, *x_loads[1:], load_q):
        copy.start()

    barrier = pltpu.get_barrier_semaphore()
    for p in peers:
        pl.semaphore_signal(barrier, inc=1, device_id=(p, tp), device_id_type=MESH)
    for p in tp_peers:
        pl.semaphore_signal(barrier, inc=1, device_id=(sp, p), device_id_type=MESH)

    tri[...] = (iota((span, span), 0) > iota((span, span), 1)).astype(F32).astype(BF16)
    for copy in small:
        copy.wait()
    eye = iota((16, 128), 0) == iota((16, 128), 1)
    bias_row = jnp.concatenate([bias[...], jnp.zeros((1, 112), F32)], axis=1)
    bias_col = jnp.sum(jnp.where(eye, bias_row, 0.0), axis=1, keepdims=True)

    def normalise(i):
        at, count = BLOCKS[i]
        total = None
        for c in range(0, width, 128):
            piece = x[at:at + count, c:c + 128].astype(F32)
            total = piece * piece if total is None else total + piece * piece
        r = lax.rsqrt(jnp.sum(total, axis=1, keepdims=True) * (1.0 / width) + EPS)
        for c in range(0, width, 128):
            xn[at:at + count, c:c + 128] = (x[at:at + count, c:c + 128].astype(F32) * r).astype(BF16)

    def project(i):
        at, count = BLOCKS[i]
        rows_n = xn[at:at + count, :]
        acc_g[at:at + count, 0:32] = lax.dot_general(
            rows_n, wg[...], (((1,), (1,)), ((), ())), preferred_element_type=F32
        )
        values[at:at + count, :] = jnp.dot(rows_n, wv[...], preferred_element_type=F32).astype(BF16)
        keys[at:at + count, :] = jnp.dot(rows_n, wk[...], preferred_element_type=F32).astype(BF16)

    x_loads[0].wait()
    normalise(0)
    for copy in w_loads:
        copy.wait()
    for i in range(1, len(BLOCKS)):
        x_loads[i].wait()
        normalise(i)
        project(i - 1)
    project(len(BLOCKS) - 1)

    gates = []
    for s in range(2):
        turned = acc_g[pl.ds(s * span, span), :].T
        gates.append((turned[0:16], log_sigmoid(turned[16:32] + bias_col)))
    parts = [split3(g[1]) for g in gates]
    lhs = jnp.concatenate([p[i] for p in parts for i in range(3)], axis=0).astype(BF16)
    after = jnp.dot(lhs, tri[...], preferred_element_type=F32)
    for s in range(2):
        igate, logf = gates[s]
        rest = after[48 * s:48 * s + 16] + after[48 * s + 16:48 * s + 32] + after[48 * s + 32:48 * s + 48]
        logw = rest + igate
        top = jnp.max(logw, axis=1, keepdims=True)
        wrow[pl.ds(16 * s, 16), :] = jnp.exp(logw - top)
        stat[0, pl.ds(16 * s, 16), :] = jnp.broadcast_to(rest[:, 0:1] + logf[:, 0:1], (16, 128))
        stat[1, pl.ds(16 * s, 16), :] = jnp.broadcast_to(top, (16, 128))

    lane = iota((1, 128), 1)
    lane_q = jnp.where(lane < 16, lane // 4, jnp.where(lane < MSG, lax.rem(lane, 4), -1))
    for i in range(2):
        line = jnp.zeros((1, 128), F32)
        for q in range(4):
            own = stat[i, pl.ds(16 * (q // 2) + 2 * tp + q % 2, 1), :]
            line = jnp.where(lane_q == q, own, line)
        send_s[pl.ds(i, 1), :] = line
    recv_s[sp] = send_s[...]

    pl.semaphore_wait(barrier, SP - 1 + TP - 1)
    s_copies, m_copies, n_copies = [], [], []
    for p in peers:
        copy = pltpu.make_async_remote_copy(
            src_ref=send_s, dst_ref=recv_s.at[sp], send_sem=ssem.at[0], recv_sem=ssem.at[1],
            device_id=(p, tp), device_id_type=MESH,
        )
        copy.start()
    for p in tp_peers:
        copy = pltpu.make_async_remote_copy(
            src_ref=fresh.at[tp], dst_ref=fresh.at[tp], send_sem=new_sem.at[0], recv_sem=new_sem.at[1],
            device_id=(sp, p), device_id_type=MESH,
        )
        copy.start()

    mats, nrms = [], []
    for q in range(4):
        s, h = q // 2, q % 2
        w = wrow[pl.ds(16 * s + 2 * tp + h, 1), :]
        block, cols = pl.ds(s * span, span), slice(h * DH, (h + 1) * DH)
        turned = (values[block, cols].T.astype(F32) * w).astype(BF16)
        hi, mid, low = split3(w)
        row = iota((16, span), 0)
        extra = jnp.where(row == 0, hi, jnp.where(row == 1, mid, jnp.where(row == 2, low, 0.0)))
        out = jnp.dot(
            jnp.concatenate([turned, extra.astype(BF16)], axis=0),
            keys[block, cols],
            preferred_element_type=F32,
        )
        mats.append(out[0:128].reshape(16, 8, 128))
        nrms.append(out[128:129] + out[129:130] + out[130:131])

    low_half = iota((16, 8, 128), 1) < 4
    evens, odds = [], []
    for a, b in ((mats[0], mats[1]), (mats[2], mats[3])):
        evens.append(jnp.where(low_half, a, pltpu.roll(b, 4, 1)))
        odds.append(jnp.where(low_half, pltpu.roll(a, 4, 1), b))
    row8 = iota((8, 128), 0)
    tail = jnp.zeros((8, 128), F32)
    for q in range(4):
        hi = nrms[q].astype(BF16).astype(F32)
        tail = jnp.where(row8 == q, hi, jnp.where(row8 == 4 + q, nrms[q] - hi, tail))
    tail = jnp.broadcast_to(tail[None], (16, 8, 128))
    send_m[:, 0] = jnp.concatenate([evens[0], evens[1], tail], axis=1).astype(BF16)
    send_m[:, 1] = jnp.concatenate([odds[0], odds[1], tail], axis=1).astype(BF16)
    for p in peers:
        copy = pltpu.make_async_remote_copy(
            src_ref=send_m.at[p // 2, lax.rem(p, 2)], dst_ref=recv_m.at[sp],
            send_sem=msem.at[0], recv_sem=msem.at[1], device_id=(p, tp), device_id_type=MESH,
        )
        copy.start()
    recv_m[sp] = send_m[sp // 2, lax.rem(sp, 2)]

    got = fresh.at[pl.ds(0, TP - 1)]
    pltpu.make_async_copy(got, got, new_sem.at[1]).wait()
    pieces = [fresh[k].astype(F32) for k in range(TP)]
    fresh_row = jnp.concatenate(pieces, axis=1)
    mean = jnp.sum(fresh_row * fresh_row, axis=1, keepdims=True) * (1.0 / width)
    token = (fresh_row * lax.rsqrt(mean + EPS)).astype(BF16)
    load_q.wait()
    key = jnp.dot(token, wk[...], preferred_element_type=F32).astype(BF16).astype(F32)
    value = jnp.dot(token, wv[...], preferred_element_type=F32).astype(BF16).astype(F32)
    query = jnp.dot(token, wq[...], preferred_element_type=F32).astype(BF16).astype(F32)
    gate = lax.dot_general(token, wg[...], (((1,), (1,)), ((), ())), preferred_element_type=F32)

    def per_row(v):
        return jnp.concatenate(
            [
                jnp.broadcast_to(v[q // 2:q // 2 + 1, (q % 2) * DH:(q % 2 + 1) * DH], (4, DH))
                for q in range(4)
            ],
            axis=0,
        )

    def picked(v, at):
        return jnp.sum(jnp.where(iota((16, v.shape[1]), 1) == at, v, 0.0), axis=1, keepdims=True)

    row16 = iota((16, 1), 0)
    own_row = 4 * sp + lax.rem(row16, 4)
    head = 2 * tp + lax.rem(row16 // 4, 2)
    q_rows, k_rows, v_rows = per_row(query), per_row(key), per_row(value)
    agreement = jnp.sum(q_rows * k_rows, axis=1, keepdims=True)
    value_own = picked(v_rows, own_row)
    gate_rows = jnp.concatenate([jnp.broadcast_to(gate[s:s + 1], (8, 32)) for s in range(2)], axis=0)
    input_new = picked(gate_rows, head)
    bias_own = picked(jnp.broadcast_to(bias_row, (16, 128)), head)
    forget_new = log_sigmoid(picked(gate_rows, 16 + head) + bias_own)

    got = recv_s.at[pl.ds(0, SP - 1)]
    pltpu.make_async_copy(got, got, ssem.at[1]).wait()
    totals, tops = recv_s[:, 0, :], recv_s[:, 1, :]
    later = (iota((SP, SP), 1) > iota((SP, SP), 0)).astype(F32).astype(BF16)
    sums = jnp.dot(later, jnp.concatenate(split3(totals), axis=1).astype(BF16), preferred_element_type=F32)
    lw = sums[:, 0:128] + sums[:, 128:256] + sums[:, 256:384] + tops
    top = jnp.max(lw, axis=0, keepdims=True)
    scale = jnp.exp(lw - top)
    stacked = jnp.concatenate([scale, jnp.broadcast_to(top, (8, 128)), jnp.zeros((88, 128), F32)], axis=0)
    turned = stacked.T
    top_col = turned[0:16, SP:SP + 1]
    share = turned[0:MSG, 0:SP]
    top_next = jnp.maximum(forget_new + top_col, input_new)
    old_share = jnp.exp(forget_new + top_col - top_next)
    new_share = jnp.exp(input_new - top_next)

    got = recv_m.at[pl.ds(0, SP - 1)]
    pltpu.make_async_copy(got, got, msem.at[1]).wait()
    merged = jnp.zeros((MSG, 128), F32)
    for d in range(SP):
        merged = merged + share[:, d:d + 1] * recv_m[d].astype(F32)
    matrix = merged[0:16].astype(BF16)
    normal = merged[16:24] + pltpu.roll(merged[16:24], 4, 0)
    n_rows = jnp.concatenate([jnp.broadcast_to(normal[q:q + 1], (4, 128)) for q in range(4)], axis=0)

    factor = DH ** (-0.5)
    numer = jnp.sum(matrix.astype(F32) * q_rows, axis=1, keepdims=True)
    numer = (old_share * numer + new_share * agreement * value_own) * factor
    denom = jnp.sum(n_rows * q_rows, axis=1, keepdims=True)
    denom = (old_share * denom + new_share * agreement) * factor
    read = numer / jnp.maximum(jnp.abs(denom), 1.0)
    own_normal = picked(n_rows, own_row)

    lane16 = iota((16, 128), 1)
    table = jnp.where(lane16 == 0, own_normal, jnp.where(lane16 == 1, top_col, read))
    table = jnp.concatenate([table, jnp.zeros((112, 128), F32)], axis=0).T
    for q in range(4):
        s, h = q // 2, q % 2
        mat_out[s, h] = matrix[4 * q:4 * q + 4]
        nrm_out[s, h:h + 1, :] = table[0:1, 4 * q:4 * q + 4]
        top_out[s:s + 1, h:h + 1] = table[1:2, 4 * q:4 * q + 1]
        read_out[s, h:h + 1, :] = table[2:3, 4 * q:4 * q + 4].astype(BF16)

    sent = recv_s.at[pl.ds(0, SP - 1)]
    pltpu.make_async_copy(sent, sent, ssem.at[0]).wait()
    sent = recv_m.at[pl.ds(0, SP - 1)]
    pltpu.make_async_copy(sent, sent, msem.at[0]).wait()
    sent = fresh.at[pl.ds(0, TP - 1)]
    pltpu.make_async_copy(sent, sent, new_sem.at[0]).wait()


def shards(inputs, w_key, w_value, w_query, w_igate, w_fgate, forget_bias, new_rows):
    seqs, span, width = inputs.shape
    rows = seqs * span
    heads = w_key.shape[1] // DH
    out_shape = (
        jax.ShapeDtypeStruct((seqs, heads, DH // SP, DH), BF16),
        jax.ShapeDtypeStruct((seqs, heads, DH // SP), F32),
        jax.ShapeDtypeStruct((seqs, heads), F32),
        jax.ShapeDtypeStruct((seqs, heads, DH // SP), BF16),
    )
    hbm = pl.BlockSpec(memory_space=pl.ANY)
    vmem = pl.BlockSpec(memory_space=pltpu.VMEM)
    dma = pltpu.SemaphoreType.DMA
    return pl.pallas_call(
        kernel,
        out_shape=out_shape,
        in_specs=[hbm] * 8,
        out_specs=[vmem] * 4,
        scratch_shapes=[
            pltpu.VMEM((rows, width), BF16),
            pltpu.VMEM((rows, width), BF16),
            pltpu.VMEM((width, heads * DH), BF16),
            pltpu.VMEM((width, heads * DH), BF16),
            pltpu.VMEM((width, heads * DH), BF16),
            pltpu.VMEM((32, width), BF16),
            pltpu.VMEM((1, 16), F32),
            pltpu.VMEM((TP, seqs, width // TP), BF16),
            pltpu.VMEM((rows, heads * DH), BF16),
            pltpu.VMEM((rows, heads * DH), BF16),
            pltpu.VMEM((rows, 128), F32),
            pltpu.VMEM((span, span), BF16),
            pltpu.VMEM((2 * 16, span), F32),
            pltpu.VMEM((2, 2 * 16, 128), F32),
            pltpu.VMEM((SP // 2, 2, MSG, 128), BF16),
            pltpu.VMEM((SP, MSG, 128), BF16),
            pltpu.VMEM((2, 128), F32),
            pltpu.VMEM((SP, 2, 128), F32),
            dma((5,)),
            dma((len(BLOCKS),)),
            dma((CHUNKS, 2)),
            dma((2,)),
            dma((2,)),
            dma((2,)),
        ],
        compiler_params=pltpu.CompilerParams(
            collective_id=0, has_side_effects=True, vmem_limit_bytes=60 * 1024 * 1024
        ),
    )(
        inputs.reshape(rows, width), w_key, w_value, w_query,
        w_igate.T, w_fgate.T, forget_bias.reshape(1, -1), new_rows,
    )


def solution(mesh):
    in_specs = (
        P(None, "sp", None),
        P(None, "tp"),
        P(None, "tp"),
        P(None, "tp"),
        P(),
        P(),
        P(),
        P(None, "tp"),
    )
    out_specs = (P(None, "tp", "sp", None), P(None, "tp", "sp"), P(None, "tp"), P(None, "tp", "sp"))
    return jax.shard_map(shards, mesh=mesh, in_specs=in_specs, out_specs=out_specs, check_vma=False)
```

time: 114 us -> 31.1 us (0.27)
  starting transfers between devices: 38.5 us -> 0 us
  waiting for transfers between devices: 34.5 us -> 0 us
  matrix products: 26.4 us -> 0 us
  Pallas kernels: 0 us -> 25.2 us
  other arithmetic: 7.66 us -> 0 us
    all_to_all x6 -> x0, starting transfers between devices: 38.5 us -> none  [the longest x4 29.3 us: from_everyone(): return lax.all_to_all(copies, axis, split_axis=0, concat_axis=0, tiled=True)]
    all_to_all x6 -> x0, waiting for transfers between devices: 34.5 us -> none  [the longest x4 17.4 us: from_everyone(): return lax.all_to_all(copies, axis, split_axis=0, concat_axis=0, tiled=True)]
    dot_general x12 -> x0, matrix products: 26.4 us -> none  [the longest x1 5.4 us: shards(): jnp.einsum('spd,dc->spc', normed, w_key, preferred_element_type=jnp.float32)]
    pallas_call x0 -> x1, Pallas kernels: none -> 25.2 us  [shards(): pl.pallas_call(kernel, out_shape=out_shape, in_specs=[hbm] * 8, out_specs...]
    unnamed x13 -> x4, local copies, waits for them, and re-layouts: 0.06 us -> 4.92 us
    reduce_sum x7 -> x0, other arithmetic: 4.75 us -> none  [the longest x2 4.33 us: normalize(): jnp.mean(scaled * scaled, axis=-1, keepdims=True) + EPS]
    broadcast_in_dim x4 -> x0, local copies, waits for them, and re-layouts: 2.47 us -> none  [from_everyone(): copies = jnp.broadcast_to(value, (lax.axis_size(axis), *value.shape))]
    another operation x3 -> x0, other arithmetic: 1.65 us -> none
  transfers between devices with their start and end apart: 6 -> 0, of which waited for: 6 -> 0; matrix products, arithmetic and copies ran while one was open for 14% -> 0% of each run, Pallas kernels for 0% -> 0%
where the time goes in v1:
time: 31.1 us; the launch traced here: 30.8 us
  Pallas kernels  25.2 us (81%)
  local copies, waits for them, and re-layouts  4.92 us (16%)
  between operations  0.64 us (2%)
    pallas_call x1, Pallas kernels, shards(): pl.pallas_call(kernel, out_shape=out_shape, in_specs=[hbm] * 8, out_specs...  25.2 us
    unnamed x4, local copies, waits for them, and re-layouts  4.92 us

profile of v1, /device:TPU:1, one launch (start us, length us, event | category | flops | bytes accessed | tf_op | source)
XLA Modules:
  0.0 30.8 jit_solution(11103190455968470121)
XLA Ops:
  0.6 25.2 %shard_map.111 = (bf16[2,2,4,128]{3,2,1,0:T(4,128)(2,1)}, f32[2,2,4]{2,1,0:T(2,128)}, f32[2,2]{1,0:T(2,128)}, bf16[2,2,4]{2,1,0:T(2,128)(2,1)}) custom-call(bf16[768,4096]{1,0:T(8,128)(2,1)} %bitcast.4, bf16[4096,256]{1,0:T(8,128)(2,1)} %wk_hbm.1, bf16[4096,256]{1,0:T(8,128)(2,1)} %wv_hbm.1, bf16[4096,256]{1,0:T(8,128)(2,1)} %wq_hbm.1, ...), custom_call_target="tpu_custom_call" | custom-call | tf_op jit(solution)/shard_map/pallas_call | solution.py:300
  25.9 1.3 %copy.16 = bf16[2,2,4,128]{3,2,1,0:T(4,128)(2,1)} copy(bf16[2,2,4,128]{3,2,1,0:T(4,128)(2,1)} %get-tuple-element.8) | data formatting | bytes 8192
  27.1 1.2 %copy.17 = f32[2,2,4]{2,1,0:T(2,128)} copy(f32[2,2,4]{2,1,0:T(2,128)} %get-tuple-element.9) | data formatting | bytes 128
  28.4 1.2 %copy.18 = f32[2,2]{1,0:T(2,128)} copy(f32[2,2]{1,0:T(2,128)} %get-tuple-element.10) | data formatting | bytes 32
  29.6 1.2 %copy.19 = bf16[2,2,4]{2,1,0:T(2,128)(2,1)} copy(bf16[2,2,4]{2,1,0:T(2,128)(2,1)} %get-tuple-element.11) | data formatting | bytes 64

commit v2 on v1

--- a/solution.py
+++ b/solution.py
@@ -43,7 +43,7 @@
 
 def kernel(
     x_hbm, wk_hbm, wv_hbm, wq_hbm, wi_hbm, wf_hbm, bias_hbm, new_hbm,
-    mat_out, nrm_out, top_out, read_out,
+    packed_out,
     x, xn, wk, wv, wq, wg, bias, fresh, keys, values, acc_g, tri, wrow, stat,
     send_m, recv_m, send_s, recv_s,
     load_sem, x_sem, w_sem, new_sem, msem, ssem,
@@ -269,12 +269,8 @@
     lane16 = iota((16, 128), 1)
     table = jnp.where(lane16 == 0, own_normal, jnp.where(lane16 == 1, top_col, read))
     table = jnp.concatenate([table, jnp.zeros((112, 128), F32)], axis=0).T
-    for q in range(4):
-        s, h = q // 2, q % 2
-        mat_out[s, h] = matrix[4 * q:4 * q + 4]
-        nrm_out[s, h:h + 1, :] = table[0:1, 4 * q:4 * q + 4]
-        top_out[s:s + 1, h:h + 1] = table[1:2, 4 * q:4 * q + 1]
-        read_out[s, h:h + 1, :] = table[2:3, 4 * q:4 * q + 4].astype(BF16)
+    packed_out[0:16] = merged[0:16]
+    packed_out[16:24] = table[0:8]
 
     sent = recv_s.at[pl.ds(0, SP - 1)]
     pltpu.make_async_copy(sent, sent, ssem.at[0]).wait()
@@ -282,6 +278,16 @@
     pltpu.make_async_copy(sent, sent, msem.at[0]).wait()
     sent = fresh.at[pl.ds(0, TP - 1)]
     pltpu.make_async_copy(sent, sent, new_sem.at[0]).wait()
+
+
+def unpack(packed, mat_out, nrm_out, top_out, read_out):
+    for q in range(4):
+        s, h = q // 2, q % 2
+        lanes = slice(4 * q, 4 * q + 4)
+        mat_out[s, h] = packed[lanes].astype(BF16)
+        nrm_out[s, h:h + 1, :] = packed[16:17, lanes]
+        top_out[s:s + 1, h:h + 1] = packed[17:18, 4 * q:4 * q + 1]
+        read_out[s, h:h + 1, :] = packed[18:19, lanes].astype(BF16)
 
 
 def shards(inputs, w_key, w_value, w_query, w_igate, w_fgate, forget_bias, new_rows):
@@ -297,11 +303,11 @@
     hbm = pl.BlockSpec(memory_space=pl.ANY)
     vmem = pl.BlockSpec(memory_space=pltpu.VMEM)
     dma = pltpu.SemaphoreType.DMA
-    return pl.pallas_call(
+    packed = pl.pallas_call(
         kernel,
-        out_shape=out_shape,
+        out_shape=pltpu.VMEM((MSG, 128), F32),
         in_specs=[hbm] * 8,
-        out_specs=[vmem] * 4,
+        out_specs=vmem,
         scratch_shapes=[
             pltpu.VMEM((rows, width), BF16),
             pltpu.VMEM((rows, width), BF16),
@@ -335,6 +341,9 @@
         inputs.reshape(rows, width), w_key, w_value, w_query,
         w_igate.T, w_fgate.T, forget_bias.reshape(1, -1), new_rows,
     )
+    return pl.pallas_call(unpack, out_shape=out_shape, in_specs=[vmem], out_specs=[vmem] * 4)(
+        pltpu.with_memory_space_constraint(packed, pltpu.VMEM)
+    )
 
 
 def solution(mesh):

time: 31.1 us -> 26.1 us (0.84)
  local copies, waits for them, and re-layouts: 4.92 us -> 0 us
    unnamed x4 -> x0, local copies, waits for them, and re-layouts: 4.92 us -> none
    pallas_call x1 -> x2, Pallas kernels: 25.2 us -> 25.2 us  [the longest x1 24.5 us: shards(): pl.pallas_call(kernel, out_shape=pltpu.VMEM((MSG, 128), F32), in_specs=[h...]
where the time goes in v2:
time: 26.1 us; the launch traced here: 25.8 us
  Pallas kernels  25.2 us (97%)
  between operations  0.64 us (2%)
    pallas_call x1, Pallas kernels, shards(): pl.pallas_call(kernel, out_shape=pltpu.VMEM((MSG, 128), F32), in_specs=[h...  24.5 us
    pallas_call x1, Pallas kernels, shards(): pl.pallas_call(unpack, out_shape=out_shape, in_specs=[vmem], out_specs=[v...  0.65 us

profile of v2, /device:TPU:1, one launch (start us, length us, event | category | flops | bytes accessed | tf_op | source)
XLA Modules:
  0.0 25.8 jit_solution(10455431045382506706)
XLA Ops:
  0.6 24.5 %shard_map.111.packed = f32[24,128]{1,0:T(8,128)S(1)} custom-call(bf16[768,4096]{1,0:T(8,128)(2,1)} %bitcast.4, bf16[4096,256]{1,0:T(8,128)(2,1)} %wk_hbm.1, bf16[4096,256]{1,0:T(8,128)(2,1)} %wv_hbm.1, bf16[4096,256]{1,0:T(8,128)(2,1)} %wq_hbm.1, bf16[16,4096]{1,0:T(8,128)(2,1)} %bitcast.5, bf16[16,4096]{1,0:T(8,128)(2,1)} %bitcast.6, f32[1,16]{1,0:T(1,128)} %bitcast.7, ...), custom_call_target="tpu_custom_call" | custom-call | tf_op jit(solution)/shard_map/pallas_call | solution.py:306
  25.2 0.7 %shard_map.112 = (bf16[2,2,4,128]{3,2,1,0:T(4,128)(2,1)}, f32[2,2,4]{2,1,0:T(2,128)}, f32[2,2]{1,0:T(2,128)}, bf16[2,2,4]{2,1,0:T(2,128)(2,1)}) custom-call(f32[24,128]{1,0:T(8,128)S(1)} %shard_map.111.packed), custom_call_target="tpu_custom_call" | custom-call | tf_op jit(solution)/shard_map/pallas_call | solution.py:344

commit v3 on v2

v3 whole, which is shorter than its diff:
```python
import functools

import jax
import jax.numpy as jnp
from jax import lax
from jax.experimental import pallas as pl
from jax.experimental.pallas import tpu as pltpu
from jax.sharding import PartitionSpec as P

DH = 128
EPS = 1e-06
MESH = pl.DeviceIdType.MESH
F32 = jnp.float32
BF16 = jnp.bfloat16
NZ, NY = 8, 4
SP, TP = NZ * NY, 8
ROWS = 128
TILE = 256
MSG = 8


def peer_offsets():
    offsets = [(dz, dy) for dz in range(NZ) for dy in range(NY) if dz or dy]
    return sorted(offsets, key=lambda o: -(min(o[0], NZ - o[0]) + min(o[1], NY - o[1])))


def iota(shape, dim):
    return lax.broadcasted_iota(jnp.int32, shape, dim)


def log_sigmoid(v):
    u = jnp.exp(-jnp.abs(v))
    series = u * (1.0 - u * (0.5 - u * (1.0 / 3.0 - u * (0.25 - u * (0.2 - u * (1.0 / 6.0))))))
    return jnp.minimum(v, 0.0) - jnp.where(u < 0.03, series, jnp.log(1.0 + u))


def split3(v):
    hi = v.astype(BF16).astype(F32)
    rest = v - hi
    mid = rest.astype(BF16).astype(F32)
    return hi, mid, rest - mid


def kernel(
    x_hbm, wk_hbm, wv_hbm, wq_hbm, wi_hbm, wf_hbm, bias_hbm, new_hbm,
    packed_out,
    x, xn, wk, wv, wq, wg, bias, fresh, acc_g, tri, wrow, stat,
    send_m, recv_m, send_n, recv_n, send_s, recv_s,
    load_sem, x_sem, w_sem, new_sem, msem, nsem, ssem,
):
    sp, tp = lax.axis_index("sp"), lax.axis_index("tp")
    z, y = sp // NY, lax.rem(sp, NY)
    span, width = xn[0].shape
    per_seq = span // ROWS
    peers = []
    for dz, dy in peer_offsets():
        peers.append(lax.rem(z + dz, NZ) * NY + lax.rem(y + dy, NY))
    tp_peers = [lax.rem(tp + k, TP) for k in range(1, TP)]

    def load(hbm, vmem, sem, parts):
        each = vmem.shape[0] // parts
        copies = []
        for i in range(parts):
            part = pl.ds(i * each, each)
            copies.append(pltpu.make_async_copy(hbm.at[part], vmem.at[part], sem))
        return copies, pltpu.make_async_copy(hbm, vmem, sem)

    def start(*loads):
        for copies, _ in loads:
            for copy in copies:
                copy.start()

    def land(*loads):
        for _, whole in loads:
            whole.wait()

    small = [
        load(wi_hbm, wg.at[pl.ds(0, 16)], load_sem.at[0], 1),
        load(wf_hbm, wg.at[pl.ds(16, 16)], load_sem.at[1], 1),
        load(bias_hbm, bias, load_sem.at[2], 1),
        load(new_hbm, fresh.at[tp], load_sem.at[3], 1),
    ]
    x_loads = [
        load(x_hbm.at[pl.ds(i * ROWS, ROWS)], x[i], x_sem.at[i], 8) for i in range(2 * per_seq)
    ]
    half = width // 2
    w_loads = []
    for i in range(2):
        part = pl.ds(i * half, half)
        w_loads.append(load(wv_hbm.at[part], wv.at[part], w_sem.at[0, i], 4))
        w_loads.append(load(wk_hbm.at[part], wk.at[part], w_sem.at[1, i], 4))
    load_q = load(wq_hbm, wq, load_sem.at[4], 4)
    start(x_loads[0], *small)

    barrier = pltpu.get_barrier_semaphore()
    for p in peers:
        pl.semaphore_signal(barrier, inc=1, device_id=(p, tp), device_id_type=MESH)
    for p in tp_peers:
        pl.semaphore_signal(barrier, inc=1, device_id=(sp, p), device_id_type=MESH)
    start(*x_loads[1:3])
    tri[...] = (iota((span, span), 0) > iota((span, span), 1)).astype(F32).astype(BF16)

    def root(i, top, count):
        total = None
        for c in range(0, width, 128):
            piece = x[i][top:top + count, c:c + 128].astype(F32)
            total = piece * piece if total is None else total + piece * piece
        mean = jnp.sum(total, axis=1, keepdims=True) * (1.0 / width)
        return lax.rsqrt(mean + EPS), total

    def gate(blocks, roots):
        totals = {}
        for c in range(0, width, TILE):
            for i in blocks:
                s, at = i // per_seq, (i % per_seq) * ROWS
                normed = (x[i][:, c:c + TILE].astype(F32) * roots[i]).astype(BF16)
                xn[s][at:at + ROWS, c:c + TILE] = normed
                for half_of in range(2):
                    top = half_of * ROWS // 2
                    part = lax.dot_general(
                        normed[top:top + ROWS // 2], wg[:, c:c + TILE],
                        (((1,), (1,)), ((), ())), preferred_element_type=F32,
                    )
                    key = i, half_of
                    totals[key] = part if key not in totals else totals[key] + part
        for (i, half_of), total in totals.items():
            s, at = i // per_seq, (i % per_seq) * ROWS + half_of * ROWS // 2
            acc_g[s][at:at + ROWS // 2, 0:32] = total

    def project(s, sums, tiles, between=None):
        for t in tiles:
            rows_n = xn[s][:, t * TILE:(t + 1) * TILE]
            zero = between[t]() if between and t in between else None
            if zero is not None:
                rows_n = jnp.concatenate([rows_n[0:16] + zero, rows_n[16:]], axis=0)
            for j, w in enumerate((wv, wk)):
                part = jnp.dot(rows_n, w[t * TILE:(t + 1) * TILE, :], preferred_element_type=F32)
                sums[j] = part if sums[j] is None else sums[j] + part

    eye = iota((16, 128), 0) == iota((16, 128), 1)

    def gates(s):
        bias_col = jnp.sum(jnp.where(eye, bias_row, 0.0), axis=1, keepdims=True)
        turned = acc_g[s][...].T
        logf = log_sigmoid(turned[16:32] + bias_col)
        lhs = jnp.concatenate(split3(logf), axis=0).astype(BF16)
        after = jnp.dot(lhs, tri[...], preferred_element_type=F32)
        rest = after[0:16] + after[16:32] + after[32:48]
        logw = rest + turned[0:16]
        top = jnp.max(logw, axis=1, keepdims=True)
        wrow[pl.ds(16 * s, 16), :] = jnp.exp(logw - top)
        stat[0, pl.ds(16 * s, 16), :] = jnp.broadcast_to(rest[:, 0:1] + logf[:, 0:1], (16, 128))
        stat[1, pl.ds(16 * s, 16), :] = jnp.broadcast_to(top, (16, 128))

    def memory(s, value, key):
        mats, nrms = [], []
        for h in range(2):
            w = wrow[pl.ds(16 * s + 2 * tp + h, 1), :]
            cols = slice(h * DH, (h + 1) * DH)
            turned = (value[:, cols].T.astype(F32) * w).astype(BF16)
            hi, mid, low = split3(w)
            row = iota((16, span), 0)
            extra = jnp.where(row == 0, hi, jnp.where(row == 1, mid, jnp.where(row == 2, low, 0.0)))
            out = jnp.dot(
                jnp.concatenate([turned, extra.astype(BF16)], axis=0),
                key[:, cols],
                preferred_element_type=F32,
            )
            mats.append(out[0:128].reshape(16, 8, 128))
            nrms.append(out[128:129] + out[129:130] + out[130:131])
        low_half = iota((16, 8, 128), 1) < 4
        a, b = mats
        send_m[s][:, 0] = jnp.where(low_half, a, pltpu.roll(b, 4, 1)).astype(BF16)
        send_m[s][:, 1] = jnp.where(low_half, pltpu.roll(a, 4, 1), b).astype(BF16)
        send_n[s][...] = jnp.concatenate(nrms, axis=0)

    def send_memory(s):
        for p in peers:
            pltpu.make_async_remote_copy(
                src_ref=send_m[s].at[p // 2, lax.rem(p, 2)], dst_ref=recv_m[s].at[sp],
                send_sem=msem.at[s, 0], recv_sem=msem.at[s, 1],
                device_id=(p, tp), device_id_type=MESH,
            ).start()
            pltpu.make_async_remote_copy(
                src_ref=send_n[s], dst_ref=recv_n[s].at[sp],
                send_sem=nsem.at[s, 0], recv_sem=nsem.at[s, 1],
                device_id=(p, tp), device_id_type=MESH,
            ).start()
        recv_m[s][sp] = send_m[s][sp // 2, lax.rem(sp, 2)]
        recv_n[s][sp] = send_n[s][...]

    roots = {}
    for i in range(per_seq):
        land(x_loads[i])
        if i == 0:
            start(w_loads[0], w_loads[1])
        else:
            start(*((w_loads[2], w_loads[3]) if i == 1 else x_loads[per_seq:]))
        roots[i] = root(i, 0, ROWS)[0]
    land(*small)
    bias_row = jnp.concatenate([bias[...], jnp.zeros((1, 112), F32)], axis=1)
    gate(range(per_seq), roots)

    tiles = width // TILE
    land(*w_loads[:2])
    start(load_q)
    sums_a, sums_b = [None, None], [None, None]
    project(0, sums_a, range(tiles // 2))
    land(*w_loads[2:], *x_loads[per_seq:])
    groups = [(i, top) for i in range(per_seq, 2 * per_seq) for top in range(0, ROWS, 16)]
    found = {}

    def squares(t):
        share = len(groups) // (tiles // 2)
        zero = None
        for i, top in groups[(t - tiles // 2) * share:(t - tiles // 2 + 1) * share]:
            found[i, top], total = root(i, top, 16)
            low = jnp.minimum(total, 0.0)
            zero = low if zero is None else zero + low
        return jnp.concatenate([zero, zero], axis=1).astype(BF16)

    def with_gates(t):
        gates(0)
        return squares(t)

    between = {t: functools.partial(squares, t) for t in range(tiles // 2, tiles)}
    between[tiles - 4] = functools.partial(with_gates, tiles - 4)
    project(0, sums_a, range(tiles // 2, tiles), between)
    for i in range(per_seq, 2 * per_seq):
        roots[i] = jnp.concatenate([found[i, top] for top in range(0, ROWS, 16)], axis=0)
    value_a, key_a = (total.astype(BF16) for total in sums_a)
    gate(range(per_seq, 2 * per_seq), roots)

    def scalars():
        gates(1)
        lane = iota((1, 128), 1)
        line = jnp.zeros((1, 128), F32)
        for i in range(2):
            for q in range(4):
                own = stat[i, pl.ds(16 * (q // 2) + 2 * tp + q % 2, 1), :]
                line = jnp.where((lane >= 64 * i + 4 * q) & (lane < 64 * i + 4 * q + 4), own, line)
        send_s[...] = line
        recv_s[sp] = line

    def send_scalars():
        for p in peers:
            pltpu.make_async_remote_copy(
                src_ref=send_s, dst_ref=recv_s.at[sp], send_sem=ssem.at[0], recv_sem=ssem.at[1],
                device_id=(p, tp), device_id_type=MESH,
            ).start()

    def send_token():
        for p in tp_peers:
            pltpu.make_async_remote_copy(
                src_ref=fresh.at[tp], dst_ref=fresh.at[tp], send_sem=new_sem.at[0], recv_sem=new_sem.at[1],
                device_id=(sp, p), device_id_type=MESH,
            ).start()

    pl.semaphore_wait(barrier, SP - 1 + TP - 1)
    between = {
        2: lambda: memory(0, value_a, key_a), 6: lambda: send_memory(0), 7: scalars, 11: send_scalars,
    }
    project(1, sums_b, range(tiles), between)
    value_b, key_b = (total.astype(BF16) for total in sums_b)
    memory(1, value_b, key_b)
    send_memory(1)
    send_token()

    got = fresh.at[pl.ds(0, TP - 1)]
    pltpu.make_async_copy(got, got, new_sem.at[1]).wait()
    pieces = [fresh[k].astype(F32) for k in range(TP)]
    fresh_row = jnp.concatenate(pieces, axis=1)
    mean = jnp.sum(fresh_row * fresh_row, axis=1, keepdims=True) * (1.0 / width)
    token = (fresh_row * lax.rsqrt(mean + EPS)).astype(BF16)
    land(load_q)
    key = jnp.dot(token, wk[...], preferred_element_type=F32).astype(BF16).astype(F32)
    value = jnp.dot(token, wv[...], preferred_element_type=F32).astype(BF16).astype(F32)
    query = jnp.dot(token, wq[...], preferred_element_type=F32).astype(BF16).astype(F32)
    new_gate = lax.dot_general(token, wg[...], (((1,), (1,)), ((), ())), preferred_element_type=F32)

    def per_row(v, s):
        return jnp.concatenate(
            [jnp.broadcast_to(v[s:s + 1, h * DH:(h + 1) * DH], (4, DH)) for h in range(2)], axis=0
        )

    def picked(v, at):
        return jnp.sum(jnp.where(iota((8, v.shape[1]), 1) == at, v, 0.0), axis=1, keepdims=True)

    row8 = iota((8, 1), 0)
    own_row = 4 * sp + lax.rem(row8, 4)
    head = 2 * tp + row8 // 4
    bias_own = picked(jnp.broadcast_to(bias_row, (8, 128)), head)
    fresh_terms = []
    for s in range(2):
        q_rows, k_rows, v_rows = (per_row(v, s) for v in (query, key, value))
        agreement = jnp.sum(q_rows * k_rows, axis=1, keepdims=True)
        value_own = picked(v_rows, own_row)
        gate_rows = jnp.broadcast_to(new_gate[s:s + 1], (8, 32))
        input_new = picked(gate_rows, head)
        forget_new = log_sigmoid(picked(gate_rows, 16 + head) + bias_own)
        fresh_terms.append((q_rows, agreement, value_own, input_new, forget_new))

    got = recv_s.at[pl.ds(0, SP - 1)]
    pltpu.make_async_copy(got, got, ssem.at[1]).wait()
    arrived = recv_s[:, 0, :]
    later = (iota((SP, SP), 1) > iota((SP, SP), 0)).astype(F32).astype(BF16)
    sums = jnp.dot(later, jnp.concatenate(split3(arrived), axis=1).astype(BF16), preferred_element_type=F32)
    lw = sums[:, 0:128] + sums[:, 128:256] + sums[:, 256:384] + pltpu.roll(arrived, 64, 1)
    top = jnp.max(lw, axis=0, keepdims=True)
    scale = jnp.exp(lw - top)
    stacked = jnp.concatenate([scale, jnp.broadcast_to(top, (8, 128)), jnp.zeros((88, 128), F32)], axis=0)
    turned = stacked.T

    factor = DH ** (-0.5)
    lane8 = iota((8, 128), 1)
    table = []
    for s in range(2):
        q_rows, agreement, value_own, input_new, forget_new = fresh_terms[s]
        top_col = turned[8 * s:8 * s + 8, SP:SP + 1]
        share = turned[8 * s:8 * s + 8, 0:SP]
        top_next = jnp.maximum(forget_new + top_col, input_new)
        old_share = jnp.exp(forget_new + top_col - top_next)
        new_share = jnp.exp(input_new - top_next)
        got = recv_m[s].at[pl.ds(0, SP - 1)]
        pltpu.make_async_copy(got, got, msem.at[s, 1]).wait()
        got = recv_n[s].at[pl.ds(0, SP - 1)]
        pltpu.make_async_copy(got, got, nsem.at[s, 1]).wait()
        merged = [jnp.zeros((8, 128), F32) for _ in range(4)]
        for d in range(SP):
            merged[d % 4] = merged[d % 4] + share[:, d:d + 1] * recv_m[s][d].astype(F32)
        merged = (merged[0] + merged[1]) + (merged[2] + merged[3])
        matrix = merged.astype(BF16)
        n_rows = []
        for h in range(2):
            at = 8 * s + 4 * h
            normal = jnp.sum(scale[:, at:at + 1] * recv_n[s][:, h, :], axis=0, keepdims=True)
            n_rows.append(jnp.broadcast_to(normal, (4, 128)))
        n_rows = jnp.concatenate(n_rows, axis=0)
        numer = jnp.sum(matrix.astype(F32) * q_rows, axis=1, keepdims=True)
        numer = (old_share * numer + new_share * agreement * value_own) * factor
        denom = jnp.sum(n_rows * q_rows, axis=1, keepdims=True)
        denom = (old_share * denom + new_share * agreement) * factor
        read = numer / jnp.maximum(jnp.abs(denom), 1.0)
        own_normal = picked(n_rows, own_row)
        table.append(jnp.where(lane8 == 0, own_normal, jnp.where(lane8 == 1, top_col, read)))
        packed_out[8 * s:8 * s + 8] = merged
    packed_out[16:24] = jnp.concatenate([*table, jnp.zeros((112, 128), F32)], axis=0).T[0:8]

    sent = recv_s.at[pl.ds(0, SP - 1)]
    pltpu.make_async_copy(sent, sent, ssem.at[0]).wait()
    for s in range(2):
        sent = recv_m[s].at[pl.ds(0, SP - 1)]
        pltpu.make_async_copy(sent, sent, msem.at[s, 0]).wait()
        sent = recv_n[s].at[pl.ds(0, SP - 1)]
        pltpu.make_async_copy(sent, sent, nsem.at[s, 0]).wait()
    sent = fresh.at[pl.ds(0, TP - 1)]
    pltpu.make_async_copy(sent, sent, new_sem.at[0]).wait()


def unpack(packed, mat_out, nrm_out, top_out, read_out):
    for q in range(4):
        s, h = q // 2, q % 2
        lanes = slice(4 * q, 4 * q + 4)
        mat_out[s, h] = packed[lanes].astype(BF16)
        nrm_out[s, h:h + 1, :] = packed[16:17, lanes]
        top_out[s:s + 1, h:h + 1] = packed[17:18, 4 * q:4 * q + 1]
        read_out[s, h:h + 1, :] = packed[18:19, lanes].astype(BF16)


def shards(inputs, w_key, w_value, w_query, w_igate, w_fgate, forget_bias, new_rows):
    seqs, span, width = inputs.shape
    rows = seqs * span
    heads = w_key.shape[1] // DH
    out_shape = (
        jax.ShapeDtypeStruct((seqs, heads, DH // SP, DH), BF16),
        jax.ShapeDtypeStruct((seqs, heads, DH // SP), F32),
        jax.ShapeDtypeStruct((seqs, heads), F32),
        jax.ShapeDtypeStruct((seqs, heads, DH // SP), BF16),
    )
    hbm = pl.BlockSpec(memory_space=pl.ANY)
    vmem = pl.BlockSpec(memory_space=pltpu.VMEM)
    dma = pltpu.SemaphoreType.DMA
    packed = pl.pallas_call(
        kernel,
        out_shape=pltpu.VMEM((24, 128), F32),
        in_specs=[hbm] * 8,
        out_specs=vmem,
        scratch_shapes=[
            [pltpu.VMEM((ROWS, width), BF16) for _ in range(rows // ROWS)],
            [pltpu.VMEM((span, width), BF16) for _ in range(seqs)],
            pltpu.VMEM((width, heads * DH), BF16),
            pltpu.VMEM((width, heads * DH), BF16),
            pltpu.VMEM((width, heads * DH), BF16),
            pltpu.VMEM((32, width), BF16),
            pltpu.VMEM((1, 16), F32),
            pltpu.VMEM((TP, seqs, width // TP), BF16),
            [pltpu.VMEM((span, 128), F32) for _ in range(seqs)],
            pltpu.VMEM((span, span), BF16),
            pltpu.VMEM((2 * 16, span), F32),
            pltpu.VMEM((2, 2 * 16, 128), F32),
            [pltpu.VMEM((SP // 2, 2, MSG, 128), BF16) for _ in range(seqs)],
            [pltpu.VMEM((SP, MSG, 128), BF16) for _ in range(seqs)],
            [pltpu.VMEM((2, 128), F32) for _ in range(seqs)],
            [pltpu.VMEM((SP, 2, 128), F32) for _ in range(seqs)],
            pltpu.VMEM((1, 128), F32),
            pltpu.VMEM((SP, 1, 128), F32),
            dma((5,)),
            dma((rows // ROWS,)),
            dma((2, 2)),
            dma((2,)),
            dma((seqs, 2)),
            dma((seqs, 2)),
            dma((2,)),
        ],
        compiler_params=pltpu.CompilerParams(
            collective_id=0, has_side_effects=True, vmem_limit_bytes=60 * 1024 * 1024
        ),
    )(
        inputs.reshape(rows, width), w_key, w_value, w_query,
        w_igate.T, w_fgate.T, forget_bias.reshape(1, -1), new_rows,
    )
    return pl.pallas_call(unpack, out_shape=out_shape, in_specs=[vmem], out_specs=[vmem] * 4)(
        pltpu.with_memory_space_constraint(packed, pltpu.VMEM)
    )


def solution(mesh):
    in_specs = (
        P(None, "sp", None),
        P(None, "tp"),
        P(None, "tp"),
        P(None, "tp"),
        P(),
        P(),
        P(),
        P(None, "tp"),
    )
    out_specs = (P(None, "tp", "sp", None), P(None, "tp", "sp"), P(None, "tp"), P(None, "tp", "sp"))
    return jax.shard_map(shards, mesh=mesh, in_specs=in_specs, out_specs=out_specs, check_vma=False)
```

time: 26.1 us -> 23.3 us (0.89)
  Pallas kernels: 25.2 us -> 22.3 us
    pallas_call x1, Pallas kernels: 24.5 us -> 21.6 us  [shards(): pl.pallas_call(kernel, out_shape=pltpu.VMEM((24, 128), F32), in_specs=[hb...]
where the time goes in v3:
time: 23.3 us; the launch traced here: 22.9 us
  Pallas kernels  22.3 us (96%)
  between operations  0.64 us (3%)
    pallas_call x1, Pallas kernels, shards(): pl.pallas_call(kernel, out_shape=pltpu.VMEM((24, 128), F32), in_specs=[hb...  21.6 us
    pallas_call x1, Pallas kernels, shards(): pl.pallas_call(unpack, out_shape=out_shape, in_specs=[vmem], out_specs=[v...  0.65 us

profile of v3, /device:TPU:1, one launch (start us, length us, event | category | flops | bytes accessed | tf_op | source)
XLA Modules:
  0.0 22.9 jit_solution(4177055076760401094)
XLA Ops:
  0.6 21.6 %shard_map.111.packed = f32[24,128]{1,0:T(8,128)S(1)} custom-call(bf16[768,4096]{1,0:T(8,128)(2,1)} %bitcast.4, bf16[4096,256]{1,0:T(8,128)(2,1)} %wk_hbm.1, bf16[4096,256]{1,0:T(8,128)(2,1)} %wv_hbm.1, bf16[4096,256]{1,0:T(8,128)(2,1)} %wq_hbm.1, bf16[16,4096]{1,0:T(8,128)(2,1)} %bitcast.5, bf16[16,4096]{1,0:T(8,128)(2,1)} %bitcast.6, f32[1,16]{1,0:T(1,128)} %bitcast.7, ...), custom_call_target="tpu_custom_call" | custom-call | tf_op jit(solution)/shard_map/pallas_call | solution.py:383
  22.3 0.7 %shard_map.112 = (bf16[2,2,4,128]{3,2,1,0:T(4,128)(2,1)}, f32[2,2,4]{2,1,0:T(2,128)}, f32[2,2]{1,0:T(2,128)}, bf16[2,2,4]{2,1,0:T(2,128)(2,1)}) custom-call(f32[24,128]{1,0:T(8,128)S(1)} %shard_map.111.packed), custom_call_target="tpu_custom_call" | custom-call | tf_op jit(solution)/shard_map/pallas_call | solution.py:422

commit v4 on v3

--- a/solution.py
+++ b/solution.py
@@ -44,9 +44,9 @@
 def kernel(
     x_hbm, wk_hbm, wv_hbm, wq_hbm, wi_hbm, wf_hbm, bias_hbm, new_hbm,
     packed_out,
-    x, xn, wk, wv, wq, wg, bias, fresh, acc_g, tri, wrow, stat,
+    x, xn, w_vk, wq, wg, bias, fresh, acc_g, tri, wrow, stat,
     send_m, recv_m, send_n, recv_n, send_s, recv_s,
-    load_sem, x_sem, w_sem, new_sem, msem, nsem, ssem,
+    sems, new_sem, msem, nsem, ssem,
 ):
     sp, tp = lax.axis_index("sp"), lax.axis_index("tp")
     z, y = sp // NY, lax.rem(sp, NY)
@@ -74,23 +74,27 @@
         for _, whole in loads:
             whole.wait()
 
-    small = [
-        load(wi_hbm, wg.at[pl.ds(0, 16)], load_sem.at[0], 1),
-        load(wf_hbm, wg.at[pl.ds(16, 16)], load_sem.at[1], 1),
-        load(bias_hbm, bias, load_sem.at[2], 1),
-        load(new_hbm, fresh.at[tp], load_sem.at[3], 1),
-    ]
+    gate_load = (
+        [
+            pltpu.make_async_copy(wi_hbm, wg.at[pl.ds(0, 16)], sems.at[6]),
+            pltpu.make_async_copy(wf_hbm, wg.at[pl.ds(16, 16)], sems.at[6]),
+        ],
+        pltpu.make_async_copy(wg, wg, sems.at[6]),
+    )
+    small = [load(bias_hbm, bias, sems.at[7], 1), load(new_hbm, fresh.at[tp], sems.at[8], 1)]
     x_loads = [
-        load(x_hbm.at[pl.ds(i * ROWS, ROWS)], x[i], x_sem.at[i], 8) for i in range(2 * per_seq)
+        load(x_hbm.at[pl.ds(i * ROWS, ROWS)], x[i], sems.at[i], 8) for i in range(2 * per_seq)
     ]
     half = width // 2
     w_loads = []
     for i in range(2):
-        part = pl.ds(i * half, half)
-        w_loads.append(load(wv_hbm.at[part], wv.at[part], w_sem.at[0, i], 4))
-        w_loads.append(load(wk_hbm.at[part], wk.at[part], w_sem.at[1, i], 4))
-    load_q = load(wq_hbm, wq, load_sem.at[4], 4)
-    start(x_loads[0], *small)
+        part, w_sem = pl.ds(i * half, half), sems.at[(9, 1)[i]]
+        copies = []
+        for j, hbm in enumerate((wv_hbm, wk_hbm)):
+            copies += load(hbm.at[part], w_vk.at[j, part], w_sem, 4)[0]
+        w_loads.append((copies, pltpu.make_async_copy(w_vk.at[:, part], w_vk.at[:, part], w_sem)))
+    load_q = load(wq_hbm, wq, sems.at[2], 4)
+    start(gate_load, x_loads[0], *small)
 
     barrier = pltpu.get_barrier_semaphore()
     for p in peers:
@@ -99,6 +103,7 @@
         pl.semaphore_signal(barrier, inc=1, device_id=(sp, p), device_id_type=MESH)
     start(*x_loads[1:3])
     tri[...] = (iota((span, span), 0) > iota((span, span), 1)).astype(F32).astype(BF16)
+    start(w_loads[0])
 
     def root(i, top, count):
         total = None
@@ -108,13 +113,19 @@
         mean = jnp.sum(total, axis=1, keepdims=True) * (1.0 / width)
         return lax.rsqrt(mean + EPS), total
 
-    def gate(blocks, roots):
+    def gate(blocks, roots, squares=None, between=None):
         totals = {}
-        for c in range(0, width, TILE):
+        for t in range(width // TILE):
+            c = t * TILE
+            if between and t in between:
+                between[t]()
             for i in blocks:
                 s, at = i // per_seq, (i % per_seq) * ROWS
                 normed = (x[i][:, c:c + TILE].astype(F32) * roots[i]).astype(BF16)
                 xn[s][at:at + ROWS, c:c + TILE] = normed
+                zero = squares(t) if squares else None
+                if zero is not None:
+                    normed = jnp.concatenate([normed[0:16] + zero, normed[16:]], axis=0)
                 for half_of in range(2):
                     top = half_of * ROWS // 2
                     part = lax.dot_general(
@@ -127,14 +138,33 @@
             s, at = i // per_seq, (i % per_seq) * ROWS + half_of * ROWS // 2
             acc_g[s][at:at + ROWS // 2, 0:32] = total
 
-    def project(s, sums, tiles, between=None):
+    def squares_of(found, blocks, first, count, stride=1):
+        groups = [(i, top) for i in blocks for top in range(0, ROWS, 16)]
+        share = len(groups) // count
+
+        def squares(t):
+            at, odd = divmod(t - first, stride)
+            if odd or not 0 <= at < count:
+                return None
+            zero = None
+            for i, top in groups[at * share:(at + 1) * share]:
+                found[i, top], total = root(i, top, 16)
+                low = jnp.minimum(total, 0.0)
+                zero = low if zero is None else zero + low
+            return jnp.concatenate([zero, zero], axis=1).astype(BF16)
+
+        return squares
+
+    def project(s, sums, tiles, squares=None, between=None):
         for t in tiles:
+            if between and t in between:
+                between[t]()
             rows_n = xn[s][:, t * TILE:(t + 1) * TILE]
-            zero = between[t]() if between and t in between else None
+            zero = squares(t) if squares else None
             if zero is not None:
                 rows_n = jnp.concatenate([rows_n[0:16] + zero, rows_n[16:]], axis=0)
-            for j, w in enumerate((wv, wk)):
-                part = jnp.dot(rows_n, w[t * TILE:(t + 1) * TILE, :], preferred_element_type=F32)
+            for j in range(2):
+                part = jnp.dot(rows_n, w_vk[j, t * TILE:(t + 1) * TILE, :], preferred_element_type=F32)
                 sums[j] = part if sums[j] is None else sums[j] + part
 
     eye = iota((16, 128), 0) == iota((16, 128), 1)
@@ -152,87 +182,83 @@
         stat[0, pl.ds(16 * s, 16), :] = jnp.broadcast_to(rest[:, 0:1] + logf[:, 0:1], (16, 128))
         stat[1, pl.ds(16 * s, 16), :] = jnp.broadcast_to(top, (16, 128))
 
+    def own_weight(s, h):
+        return wrow[pl.ds(16 * s + 2 * tp + h, 1), :]
+
+    def normalizer(s, key):
+        row = iota((16, span), 0)
+        lhs = jnp.zeros((16, span), F32)
+        for h in range(2):
+            for i, part in enumerate(split3(own_weight(s, h))):
+                lhs = jnp.where(row == 3 * h + i, part, lhs)
+        out = jnp.dot(lhs.astype(BF16), key, preferred_element_type=F32)
+        send_n[s][...] = jnp.concatenate(
+            [out[0:1, 0:DH] + out[1:2, 0:DH] + out[2:3, 0:DH], out[3:4, DH:] + out[4:5, DH:] + out[5:6, DH:]], axis=0
+        )
+
     def memory(s, value, key):
-        mats, nrms = [], []
+        mats = []
         for h in range(2):
-            w = wrow[pl.ds(16 * s + 2 * tp + h, 1), :]
             cols = slice(h * DH, (h + 1) * DH)
-            turned = (value[:, cols].T.astype(F32) * w).astype(BF16)
-            hi, mid, low = split3(w)
-            row = iota((16, span), 0)
-            extra = jnp.where(row == 0, hi, jnp.where(row == 1, mid, jnp.where(row == 2, low, 0.0)))
-            out = jnp.dot(
-                jnp.concatenate([turned, extra.astype(BF16)], axis=0),
-                key[:, cols],
-                preferred_element_type=F32,
-            )
-            mats.append(out[0:128].reshape(16, 8, 128))
-            nrms.append(out[128:129] + out[129:130] + out[130:131])
+            turned = (value[:, cols].T.astype(F32) * own_weight(s, h)).astype(BF16)
+            out = jnp.dot(turned, key[:, cols], preferred_element_type=F32)
+            mats.append(out.reshape(16, 8, 128))
         low_half = iota((16, 8, 128), 1) < 4
         a, b = mats
         send_m[s][:, 0] = jnp.where(low_half, a, pltpu.roll(b, 4, 1)).astype(BF16)
         send_m[s][:, 1] = jnp.where(low_half, pltpu.roll(a, 4, 1), b).astype(BF16)
-        send_n[s][...] = jnp.concatenate(nrms, axis=0)
 
     def send_memory(s):
         for p in peers:
             pltpu.make_async_remote_copy(
                 src_ref=send_m[s].at[p // 2, lax.rem(p, 2)], dst_ref=recv_m[s].at[sp],
-                send_sem=msem.at[s, 0], recv_sem=msem.at[s, 1],
+                send_sem=sems.at[3 + s], recv_sem=msem.at[s],
                 device_id=(p, tp), device_id_type=MESH,
             ).start()
             pltpu.make_async_remote_copy(
                 src_ref=send_n[s], dst_ref=recv_n[s].at[sp],
-                send_sem=nsem.at[s, 0], recv_sem=nsem.at[s, 1],
+                send_sem=sems.at[5 + s], recv_sem=nsem.at[s],
                 device_id=(p, tp), device_id_type=MESH,
             ).start()
         recv_m[s][sp] = send_m[s][sp // 2, lax.rem(sp, 2)]
         recv_n[s][sp] = send_n[s][...]
 
-    roots = {}
-    for i in range(per_seq):
-        land(x_loads[i])
-        if i == 0:
-            start(w_loads[0], w_loads[1])
-        else:
-            start(*((w_loads[2], w_loads[3]) if i == 1 else x_loads[per_seq:]))
-        roots[i] = root(i, 0, ROWS)[0]
-    land(*small)
+    tiles = width // TILE
+    roots, found = {}, {}
+
+    def collected(i):
+        roots[i] = jnp.concatenate([found[i, top] for top in range(0, ROWS, 16)], axis=0)
+
+    land(x_loads[0])
+    start(*x_loads[3:5])
+    roots[0] = root(0, 0, ROWS)[0]
+    land(gate_load, x_loads[1], *small)
+    start(w_loads[1], x_loads[5])
     bias_row = jnp.concatenate([bias[...], jnp.zeros((1, 112), F32)], axis=1)
-    gate(range(per_seq), roots)
-
-    tiles = width // TILE
-    land(*w_loads[:2])
+    gate([0], roots, squares_of(found, [1], 0, 8, 2))
+    collected(1)
+    land(x_loads[2])
+    gate([1], roots, squares_of(found, [2], 0, 8, 2))
+    collected(2)
+    gate([2], roots)
+
+    land(w_loads[0], *x_loads[3:5])
     start(load_q)
     sums_a, sums_b = [None, None], [None, None]
-    project(0, sums_a, range(tiles // 2))
-    land(*w_loads[2:], *x_loads[per_seq:])
-    groups = [(i, top) for i in range(per_seq, 2 * per_seq) for top in range(0, ROWS, 16)]
-    found = {}
-
-    def squares(t):
-        share = len(groups) // (tiles // 2)
-        zero = None
-        for i, top in groups[(t - tiles // 2) * share:(t - tiles // 2 + 1) * share]:
-            found[i, top], total = root(i, top, 16)
-            low = jnp.minimum(total, 0.0)
-            zero = low if zero is None else zero + low
-        return jnp.concatenate([zero, zero], axis=1).astype(BF16)
-
-    def with_gates(t):
-        gates(0)
-        return squares(t)
-
-    between = {t: functools.partial(squares, t) for t in range(tiles // 2, tiles)}
-    between[tiles - 4] = functools.partial(with_gates, tiles - 4)
-    project(0, sums_a, range(tiles // 2, tiles), between)
+    project(0, sums_a, range(tiles // 2), squares_of(found, [3, 4], 0, 8))
+    land(w_loads[1], x_loads[5])
+    pl.semaphore_wait(barrier, SP - 1 + TP - 1)
+    project(0, sums_a, range(tiles // 2, tiles), squares_of(found, [5], tiles // 2, 8))
     for i in range(per_seq, 2 * per_seq):
-        roots[i] = jnp.concatenate([found[i, top] for top in range(0, ROWS, 16)], axis=0)
+        collected(i)
     value_a, key_a = (total.astype(BF16) for total in sums_a)
-    gate(range(per_seq, 2 * per_seq), roots)
+    def first_memory():
+        memory(0, value_a, key_a)
+        normalizer(0, key_a)
+
+    gate(range(per_seq, 2 * per_seq), roots, None, {8: lambda: gates(0)})
 
     def scalars():
-        gates(1)
         lane = iota((1, 128), 1)
         line = jnp.zeros((1, 128), F32)
         for i in range(2):
@@ -245,36 +271,36 @@
     def send_scalars():
         for p in peers:
             pltpu.make_async_remote_copy(
-                src_ref=send_s, dst_ref=recv_s.at[sp], send_sem=ssem.at[0], recv_sem=ssem.at[1],
+                src_ref=send_s, dst_ref=recv_s.at[sp], send_sem=sems.at[7], recv_sem=ssem,
                 device_id=(p, tp), device_id_type=MESH,
             ).start()
 
     def send_token():
         for p in tp_peers:
             pltpu.make_async_remote_copy(
-                src_ref=fresh.at[tp], dst_ref=fresh.at[tp], send_sem=new_sem.at[0], recv_sem=new_sem.at[1],
+                src_ref=fresh.at[tp], dst_ref=fresh.at[tp], send_sem=sems.at[8], recv_sem=new_sem,
                 device_id=(sp, p), device_id_type=MESH,
             ).start()
 
-    pl.semaphore_wait(barrier, SP - 1 + TP - 1)
     between = {
-        2: lambda: memory(0, value_a, key_a), 6: lambda: send_memory(0), 7: scalars, 11: send_scalars,
+        1: send_token, 2: first_memory, 6: lambda: send_memory(0), 7: lambda: gates(1), 8: scalars, 11: send_scalars,
     }
-    project(1, sums_b, range(tiles), between)
+    project(1, sums_b, range(tiles), None, between)
     value_b, key_b = (total.astype(BF16) for total in sums_b)
+    normalizer(1, key_b)
     memory(1, value_b, key_b)
     send_memory(1)
-    send_token()
 
     got = fresh.at[pl.ds(0, TP - 1)]
-    pltpu.make_async_copy(got, got, new_sem.at[1]).wait()
+    pltpu.make_async_copy(got, got, sems.at[8]).wait()
+    pltpu.make_async_copy(got, got, new_sem).wait()
     pieces = [fresh[k].astype(F32) for k in range(TP)]
     fresh_row = jnp.concatenate(pieces, axis=1)
     mean = jnp.sum(fresh_row * fresh_row, axis=1, keepdims=True) * (1.0 / width)
     token = (fresh_row * lax.rsqrt(mean + EPS)).astype(BF16)
     land(load_q)
-    key = jnp.dot(token, wk[...], preferred_element_type=F32).astype(BF16).astype(F32)
-    value = jnp.dot(token, wv[...], preferred_element_type=F32).astype(BF16).astype(F32)
+    key = jnp.dot(token, w_vk[1], preferred_element_type=F32).astype(BF16).astype(F32)
+    value = jnp.dot(token, w_vk[0], preferred_element_type=F32).astype(BF16).astype(F32)
     query = jnp.dot(token, wq[...], preferred_element_type=F32).astype(BF16).astype(F32)
     new_gate = lax.dot_general(token, wg[...], (((1,), (1,)), ((), ())), preferred_element_type=F32)
 
@@ -301,7 +327,8 @@
         fresh_terms.append((q_rows, agreement, value_own, input_new, forget_new))
 
     got = recv_s.at[pl.ds(0, SP - 1)]
-    pltpu.make_async_copy(got, got, ssem.at[1]).wait()
+    pltpu.make_async_copy(got, got, sems.at[7]).wait()
+    pltpu.make_async_copy(got, got, ssem).wait()
     arrived = recv_s[:, 0, :]
     later = (iota((SP, SP), 1) > iota((SP, SP), 0)).astype(F32).astype(BF16)
     sums = jnp.dot(later, jnp.concatenate(split3(arrived), axis=1).astype(BF16), preferred_element_type=F32)
@@ -321,19 +348,22 @@
         top_next = jnp.maximum(forget_new + top_col, input_new)
         old_share = jnp.exp(forget_new + top_col - top_next)
         new_share = jnp.exp(input_new - top_next)
+        shares = [jnp.broadcast_to(share[:, d:d + 1], (8, 128)) for d in range(SP)]
+        scales = [jnp.broadcast_to(scale[:, 8 * s + 4 * h:8 * s + 4 * h + 1], (SP, 128)) for h in range(2)]
         got = recv_m[s].at[pl.ds(0, SP - 1)]
-        pltpu.make_async_copy(got, got, msem.at[s, 1]).wait()
+        pltpu.make_async_copy(got, got, sems.at[3 + s]).wait()
+        pltpu.make_async_copy(got, got, msem.at[s]).wait()
         got = recv_n[s].at[pl.ds(0, SP - 1)]
-        pltpu.make_async_copy(got, got, nsem.at[s, 1]).wait()
+        pltpu.make_async_copy(got, got, sems.at[5 + s]).wait()
+        pltpu.make_async_copy(got, got, nsem.at[s]).wait()
         merged = [jnp.zeros((8, 128), F32) for _ in range(4)]
         for d in range(SP):
-            merged[d % 4] = merged[d % 4] + share[:, d:d + 1] * recv_m[s][d].astype(F32)
+            merged[d % 4] = merged[d % 4] + shares[d] * recv_m[s][d].astype(F32)
         merged = (merged[0] + merged[1]) + (merged[2] + merged[3])
         matrix = merged.astype(BF16)
         n_rows = []
         for h in range(2):
-            at = 8 * s + 4 * h
-            normal = jnp.sum(scale[:, at:at + 1] * recv_n[s][:, h, :], axis=0, keepdims=True)
+            normal = jnp.sum(scales[h] * recv_n[s][:, h, :], axis=0, keepdims=True)
             n_rows.append(jnp.broadcast_to(normal, (4, 128)))
         n_rows = jnp.concatenate(n_rows, axis=0)
         numer = jnp.sum(matrix.astype(F32) * q_rows, axis=1, keepdims=True)
@@ -345,16 +375,6 @@
         table.append(jnp.where(lane8 == 0, own_normal, jnp.where(lane8 == 1, top_col, read)))
         packed_out[8 * s:8 * s + 8] = merged
     packed_out[16:24] = jnp.concatenate([*table, jnp.zeros((112, 128), F32)], axis=0).T[0:8]
-
-    sent = recv_s.at[pl.ds(0, SP - 1)]
-    pltpu.make_async_copy(sent, sent, ssem.at[0]).wait()
-    for s in range(2):
-        sent = recv_m[s].at[pl.ds(0, SP - 1)]
-        pltpu.make_async_copy(sent, sent, msem.at[s, 0]).wait()
-        sent = recv_n[s].at[pl.ds(0, SP - 1)]
-        pltpu.make_async_copy(sent, sent, nsem.at[s, 0]).wait()
-    sent = fresh.at[pl.ds(0, TP - 1)]
-    pltpu.make_async_copy(sent, sent, new_sem.at[0]).wait()
 
 
 def unpack(packed, mat_out, nrm_out, top_out, read_out):
@@ -388,8 +408,7 @@
         scratch_shapes=[
             [pltpu.VMEM((ROWS, width), BF16) for _ in range(rows // ROWS)],
             [pltpu.VMEM((span, width), BF16) for _ in range(seqs)],
-            pltpu.VMEM((width, heads * DH), BF16),
-            pltpu.VMEM((width, heads * DH), BF16),
+            pltpu.VMEM((2, width, heads * DH), BF16),
             pltpu.VMEM((width, heads * DH), BF16),
             pltpu.VMEM((32, width), BF16),
             pltpu.VMEM((1, 16), F32),
@@ -404,13 +423,11 @@
             [pltpu.VMEM((SP, 2, 128), F32) for _ in range(seqs)],
             pltpu.VMEM((1, 128), F32),
             pltpu.VMEM((SP, 1, 128), F32),
-            dma((5,)),
-            dma((rows // ROWS,)),
-            dma((2, 2)),
-            dma((2,)),
-            dma((seqs, 2)),
-            dma((seqs, 2)),
-            dma((2,)),
+            dma((10,)),
+            dma,
+            dma((seqs,)),
+            dma((seqs,)),
+            dma,
         ],
         compiler_params=pltpu.CompilerParams(
             collective_id=0, has_side_effects=True, vmem_limit_bytes=60 * 1024 * 1024

time: 23.3 us -> 22.3 us (0.957); the launches traced: 22.9 us -> 22.2 us
  Pallas kernels: 22.3 us -> 21.6 us
    pallas_call x1, Pallas kernels: 21.6 us -> 20.9 us  [shards(): pl.pallas_call(kernel, out_shape=pltpu.VMEM((24, 128), F32), in_specs=[hb...]
where the time goes in v4:
time: 22.3 us; the launch traced here: 22.2 us
  Pallas kernels  21.6 us (97%)
  between operations  0.64 us (3%)
    pallas_call x1, Pallas kernels, shards(): pl.pallas_call(kernel, out_shape=pltpu.VMEM((24, 128), F32), in_specs=[hb...  20.9 us
    pallas_call x1, Pallas kernels, shards(): pl.pallas_call(unpack, out_shape=out_shape, in_specs=[vmem], out_specs=[v...  0.65 us

profile of v4, /device:TPU:1, one launch (start us, length us, event | category | flops | bytes accessed | tf_op | source)
XLA Modules:
  0.0 22.2 jit_solution(13134464127746950551)
XLA Ops:
  0.6 20.9 %shard_map.111.packed = f32[24,128]{1,0:T(8,128)S(1)} custom-call(bf16[768,4096]{1,0:T(8,128)(2,1)} %bitcast.4, bf16[4096,256]{1,0:T(8,128)(2,1)} %wk_hbm.1, bf16[4096,256]{1,0:T(8,128)(2,1)} %wv_hbm.1, bf16[4096,256]{1,0:T(8,128)(2,1)} %wq_hbm.1, bf16[16,4096]{1,0:T(8,128)(2,1)} %bitcast.5, bf16[16,4096]{1,0:T(8,128)(2,1)} %bitcast.6, f32[1,16]{1,0:T(1,128)} %bitcast.7, ...), custom_call_target="tpu_custom_call" | custom-call | tf_op jit(solution)/shard_map/pallas_call | solution.py:403
  21.5 0.7 %shard_map.112 = (bf16[2,2,4,128]{3,2,1,0:T(4,128)(2,1)}, f32[2,2,4]{2,1,0:T(2,128)}, f32[2,2]{1,0:T(2,128)}, bf16[2,2,4]{2,1,0:T(2,128)(2,1)}) custom-call(f32[24,128]{1,0:T(8,128)S(1)} %shard_map.111.packed), custom_call_target="tpu_custom_call" | custom-call | tf_op jit(solution)/shard_map/pallas_call | solution.py:439

commit v5 on v4

--- a/solution.py
+++ b/solution.py
@@ -44,17 +44,20 @@
 def kernel(
     x_hbm, wk_hbm, wv_hbm, wq_hbm, wi_hbm, wf_hbm, bias_hbm, new_hbm,
     packed_out,
-    x, xn, w_vk, wq, wg, bias, fresh, acc_g, tri, wrow, stat,
+    x, xn, w_vk, wq, wg, bias, fresh, acc_g, tri, wrow, mate_out, mate_in, table,
     send_m, recv_m, send_n, recv_n, send_s, recv_s,
-    sems, new_sem, msem, nsem, ssem,
+    sems, mate_sem, new_sem, msem, nsem, ssem,
 ):
     sp, tp = lax.axis_index("sp"), lax.axis_index("tp")
     z, y = sp // NY, lax.rem(sp, NY)
-    span, width = xn[0].shape
+    span, width = xn.shape
     per_seq = span // ROWS
     peers = []
     for dz, dy in peer_offsets():
         peers.append(lax.rem(z + dz, NZ) * NY + lax.rem(y + dy, NY))
+    core = lax.rem(tp, 2)
+    order = core, 1 - core
+    mate = tp + 1 - 2 * core
     tp_peers = [lax.rem(tp + k, TP) for k in range(1, TP)]
 
     def load(hbm, vmem, sem, parts):
@@ -83,7 +86,11 @@
     )
     small = [load(bias_hbm, bias, sems.at[7], 1), load(new_hbm, fresh.at[tp], sems.at[8], 1)]
     x_loads = [
-        load(x_hbm.at[pl.ds(i * ROWS, ROWS)], x[i], sems.at[i], 8) for i in range(2 * per_seq)
+        load(
+            x_hbm.at[pl.ds(pl.multiple_of(order[i // per_seq] * span + i % per_seq * ROWS, ROWS), ROWS)],
+            x[i], sems.at[i], 8,
+        )
+        for i in range(2 * per_seq)
     ]
     half = width // 2
     w_loads = []
@@ -120,9 +127,9 @@
             if between and t in between:
                 between[t]()
             for i in blocks:
-                s, at = i // per_seq, (i % per_seq) * ROWS
+                at = i * ROWS
                 normed = (x[i][:, c:c + TILE].astype(F32) * roots[i]).astype(BF16)
-                xn[s][at:at + ROWS, c:c + TILE] = normed
+                xn[at:at + ROWS, c:c + TILE] = normed
                 zero = squares(t) if squares else None
                 if zero is not None:
                     normed = jnp.concatenate([normed[0:16] + zero, normed[16:]], axis=0)
@@ -135,8 +142,8 @@
                     key = i, half_of
                     totals[key] = part if key not in totals else totals[key] + part
         for (i, half_of), total in totals.items():
-            s, at = i // per_seq, (i % per_seq) * ROWS + half_of * ROWS // 2
-            acc_g[s][at:at + ROWS // 2, 0:32] = total
+            at = i * ROWS + half_of * ROWS // 2
+            acc_g[at:at + ROWS // 2, 0:32] = total
 
     def squares_of(found, blocks, first, count, stride=1):
         groups = [(i, top) for i in blocks for top in range(0, ROWS, 16)]
@@ -155,11 +162,11 @@
 
         return squares
 
-    def project(s, sums, tiles, squares=None, between=None):
+    def project(normed, sums, tiles, squares=None, between=None):
         for t in tiles:
             if between and t in between:
                 between[t]()
-            rows_n = xn[s][:, t * TILE:(t + 1) * TILE]
+            rows_n = normed(t)
             zero = squares(t) if squares else None
             if zero is not None:
                 rows_n = jnp.concatenate([rows_n[0:16] + zero, rows_n[16:]], axis=0)
@@ -167,23 +174,40 @@
                 part = jnp.dot(rows_n, w_vk[j, t * TILE:(t + 1) * TILE, :], preferred_element_type=F32)
                 sums[j] = part if sums[j] is None else sums[j] + part
 
+    def first_rows(t):
+        return xn[:, t * TILE:(t + 1) * TILE]
+
+    def second_rows(t):
+        return jnp.concatenate(
+            [
+                (x[i][:, t * TILE:(t + 1) * TILE].astype(F32) * roots[i]).astype(BF16)
+                for i in range(per_seq, 2 * per_seq)
+            ],
+            axis=0,
+        )
+
     eye = iota((16, 128), 0) == iota((16, 128), 1)
 
-    def gates(s):
+    def gates():
         bias_col = jnp.sum(jnp.where(eye, bias_row, 0.0), axis=1, keepdims=True)
-        turned = acc_g[s][...].T
+        turned = acc_g[...].T
         logf = log_sigmoid(turned[16:32] + bias_col)
         lhs = jnp.concatenate(split3(logf), axis=0).astype(BF16)
         after = jnp.dot(lhs, tri[...], preferred_element_type=F32)
         rest = after[0:16] + after[16:32] + after[32:48]
         logw = rest + turned[0:16]
         top = jnp.max(logw, axis=1, keepdims=True)
-        wrow[pl.ds(16 * s, 16), :] = jnp.exp(logw - top)
-        stat[0, pl.ds(16 * s, 16), :] = jnp.broadcast_to(rest[:, 0:1] + logf[:, 0:1], (16, 128))
-        stat[1, pl.ds(16 * s, 16), :] = jnp.broadcast_to(top, (16, 128))
+        wrow[:, 0:span] = jnp.exp(logw - top)
+        wrow[:, span:span + 128] = jnp.broadcast_to(rest[:, 0:1] + logf[:, 0:1], (16, 128))
+        wrow[:, span + 128:span + 256] = jnp.broadcast_to(top, (16, 128))
+        for h in range(2):
+            mate_out[h:h + 1, :] = wrow[pl.ds(2 * mate + h, 1), :]
+
+    def own_row_of(s, h):
+        return wrow[pl.ds(2 * tp + h, 1), :] if s == 0 else mate_in[h:h + 1, :]
 
     def own_weight(s, h):
-        return wrow[pl.ds(16 * s + 2 * tp + h, 1), :]
+        return own_row_of(s, h)[:, 0:span]
 
     def normalizer(s, key):
         row = iota((16, span), 0)
@@ -245,25 +269,42 @@
     land(w_loads[0], *x_loads[3:5])
     start(load_q)
     sums_a, sums_b = [None, None], [None, None]
-    project(0, sums_a, range(tiles // 2), squares_of(found, [3, 4], 0, 8))
+    project(first_rows, sums_a, range(tiles // 2), squares_of(found, [3, 4], 0, 8), {5: gates})
     land(w_loads[1], x_loads[5])
-    pl.semaphore_wait(barrier, SP - 1 + TP - 1)
-    project(0, sums_a, range(tiles // 2, tiles), squares_of(found, [5], tiles // 2, 8))
+    handed = []
+
+    def greet_and_hand():
+        pl.semaphore_wait(barrier, SP - 1 + TP - 1)
+        handed.append(pltpu.make_async_remote_copy(
+            src_ref=mate_out, dst_ref=mate_in, send_sem=sems.at[9], recv_sem=mate_sem,
+            device_id=(sp, mate), device_id_type=MESH,
+        ))
+        handed[0].start()
+
+    def send_token():
+        for p in tp_peers:
+            pltpu.make_async_remote_copy(
+                src_ref=fresh.at[tp], dst_ref=fresh.at[tp], send_sem=sems.at[8], recv_sem=new_sem,
+                device_id=(sp, p), device_id_type=MESH,
+            ).start()
+
+    project(
+        first_rows, sums_a, range(tiles // 2, tiles), squares_of(found, [5], tiles // 2, 8)
+    )
     for i in range(per_seq, 2 * per_seq):
         collected(i)
     value_a, key_a = (total.astype(BF16) for total in sums_a)
+
     def first_memory():
         memory(0, value_a, key_a)
         normalizer(0, key_a)
-
-    gate(range(per_seq, 2 * per_seq), roots, None, {8: lambda: gates(0)})
 
     def scalars():
         lane = iota((1, 128), 1)
         line = jnp.zeros((1, 128), F32)
         for i in range(2):
             for q in range(4):
-                own = stat[i, pl.ds(16 * (q // 2) + 2 * tp + q % 2, 1), :]
+                own = own_row_of(q // 2, q % 2)[:, span + 128 * i:span + 128 * (i + 1)]
                 line = jnp.where((lane >= 64 * i + 4 * q) & (lane < 64 * i + 4 * q + 4), own, line)
         send_s[...] = line
         recv_s[sp] = line
@@ -275,17 +316,12 @@
                 device_id=(p, tp), device_id_type=MESH,
             ).start()
 
-    def send_token():
-        for p in tp_peers:
-            pltpu.make_async_remote_copy(
-                src_ref=fresh.at[tp], dst_ref=fresh.at[tp], send_sem=sems.at[8], recv_sem=new_sem,
-                device_id=(sp, p), device_id_type=MESH,
-            ).start()
-
-    between = {
-        1: send_token, 2: first_memory, 6: lambda: send_memory(0), 7: lambda: gates(1), 8: scalars, 11: send_scalars,
-    }
-    project(1, sums_b, range(tiles), None, between)
+    def arrived_scalars():
+        handed[0].wait()
+        scalars()
+
+    between = {2: first_memory, 4: greet_and_hand, 5: lambda: send_memory(0), 9: send_token, 11: arrived_scalars, 13: send_scalars}
+    project(second_rows, sums_b, range(tiles), None, between)
     value_b, key_b = (total.astype(BF16) for total in sums_b)
     normalizer(1, key_b)
     memory(1, value_b, key_b)
@@ -304,9 +340,12 @@
     query = jnp.dot(token, wq[...], preferred_element_type=F32).astype(BF16).astype(F32)
     new_gate = lax.dot_general(token, wg[...], (((1,), (1,)), ((), ())), preferred_element_type=F32)
 
+    def of_prompt(v, s):
+        return jnp.where(order[s] == 0, v[0:1], v[1:2])
+
     def per_row(v, s):
         return jnp.concatenate(
-            [jnp.broadcast_to(v[s:s + 1, h * DH:(h + 1) * DH], (4, DH)) for h in range(2)], axis=0
+            [jnp.broadcast_to(of_prompt(v, s)[:, h * DH:(h + 1) * DH], (4, DH)) for h in range(2)], axis=0
         )
 
     def picked(v, at):
@@ -321,7 +360,7 @@
         q_rows, k_rows, v_rows = (per_row(v, s) for v in (query, key, value))
         agreement = jnp.sum(q_rows * k_rows, axis=1, keepdims=True)
         value_own = picked(v_rows, own_row)
-        gate_rows = jnp.broadcast_to(new_gate[s:s + 1], (8, 32))
+        gate_rows = jnp.broadcast_to(of_prompt(new_gate, s), (8, 32))
         input_new = picked(gate_rows, head)
         forget_new = log_sigmoid(picked(gate_rows, 16 + head) + bias_own)
         fresh_terms.append((q_rows, agreement, value_own, input_new, forget_new))
@@ -340,7 +379,6 @@
 
     factor = DH ** (-0.5)
     lane8 = iota((8, 128), 1)
-    table = []
     for s in range(2):
         q_rows, agreement, value_own, input_new, forget_new = fresh_terms[s]
         top_col = turned[8 * s:8 * s + 8, SP:SP + 1]
@@ -372,9 +410,10 @@
         denom = (old_share * denom + new_share * agreement) * factor
         read = numer / jnp.maximum(jnp.abs(denom), 1.0)
         own_normal = picked(n_rows, own_row)
-        table.append(jnp.where(lane8 == 0, own_normal, jnp.where(lane8 == 1, top_col, read)))
-        packed_out[8 * s:8 * s + 8] = merged
-    packed_out[16:24] = jnp.concatenate([*table, jnp.zeros((112, 128), F32)], axis=0).T[0:8]
+        at = pl.ds(pl.multiple_of(8 * order[s], 8), 8)
+        table[at, :] = jnp.where(lane8 == 0, own_normal, jnp.where(lane8 == 1, top_col, read))
+        packed_out[at, :] = merged
+    packed_out[16:24] = jnp.concatenate([table[...], jnp.zeros((112, 128), F32)], axis=0).T[0:8]
 
 
 def unpack(packed, mat_out, nrm_out, top_out, read_out):
@@ -407,16 +446,18 @@
         out_specs=vmem,
         scratch_shapes=[
             [pltpu.VMEM((ROWS, width), BF16) for _ in range(rows // ROWS)],
-            [pltpu.VMEM((span, width), BF16) for _ in range(seqs)],
+            pltpu.VMEM((span, width), BF16),
             pltpu.VMEM((2, width, heads * DH), BF16),
             pltpu.VMEM((width, heads * DH), BF16),
             pltpu.VMEM((32, width), BF16),
             pltpu.VMEM((1, 16), F32),
             pltpu.VMEM((TP, seqs, width // TP), BF16),
-            [pltpu.VMEM((span, 128), F32) for _ in range(seqs)],
+            pltpu.VMEM((span, 128), F32),
             pltpu.VMEM((span, span), BF16),
-            pltpu.VMEM((2 * 16, span), F32),
-            pltpu.VMEM((2, 2 * 16, 128), F32),
+            pltpu.VMEM((16, span + 256), F32),
+            pltpu.VMEM((2, span + 256), F32),
+            pltpu.VMEM((2, span + 256), F32),
+            pltpu.VMEM((16, 128), F32),
             [pltpu.VMEM((SP // 2, 2, MSG, 128), BF16) for _ in range(seqs)],
             [pltpu.VMEM((SP, MSG, 128), BF16) for _ in range(seqs)],
             [pltpu.VMEM((2, 128), F32) for _ in range(seqs)],
@@ -424,6 +465,7 @@
             pltpu.VMEM((1, 128), F32),
             pltpu.VMEM((SP, 1, 128), F32),
             dma((10,)),
+            dma,
             dma,
             dma((seqs,)),
             dma((seqs,)),

time: 22.3 us -> 21.9 us (0.982)
  Pallas kernels: 21.6 us -> 21.2 us
    pallas_call x1, Pallas kernels: 20.9 us -> 20.6 us  [shards(): pl.pallas_call(kernel, out_shape=pltpu.VMEM((24, 128), F32), in_specs=[hb...]
where the time goes in v5:
time: 21.9 us
  Pallas kernels  21.2 us (97%)
  between operations  0.64 us (3%)
    pallas_call x1, Pallas kernels, shards(): pl.pallas_call(kernel, out_shape=pltpu.VMEM((24, 128), F32), in_specs=[hb...  20.6 us
    pallas_call x1, Pallas kernels, shards(): pl.pallas_call(unpack, out_shape=out_shape, in_specs=[vmem], out_specs=[v...  0.65 us

profile of v5, /device:TPU:1, one launch (start us, length us, event | category | flops | bytes accessed | tf_op | source)
XLA Modules:
  0.0 21.9 jit_solution(4659777065354878775)
XLA Ops:
  0.6 20.6 %shard_map.111.packed = f32[24,128]{1,0:T(8,128)S(1)} custom-call(bf16[768,4096]{1,0:T(8,128)(2,1)} %bitcast.4, bf16[4096,256]{1,0:T(8,128)(2,1)} %wk_hbm.1, bf16[4096,256]{1,0:T(8,128)(2,1)} %wv_hbm.1, bf16[4096,256]{1,0:T(8,128)(2,1)} %wq_hbm.1, bf16[16,4096]{1,0:T(8,128)(2,1)} %bitcast.5, bf16[16,4096]{1,0:T(8,128)(2,1)} %bitcast.6, f32[1,16]{1,0:T(1,128)} %bitcast.7, ...), custom_call_target="tpu_custom_call" | custom-call | tf_op jit(solution)/shard_map/pallas_call | solution.py:442
  21.2 0.7 %shard_map.112 = (bf16[2,2,4,128]{3,2,1,0:T(4,128)(2,1)}, f32[2,2,4]{2,1,0:T(2,128)}, f32[2,2]{1,0:T(2,128)}, bf16[2,2,4]{2,1,0:T(2,128)(2,1)}) custom-call(f32[24,128]{1,0:T(8,128)S(1)} %shard_map.111.packed), custom_call_target="tpu_custom_call" | custom-call | tf_op jit(solution)/shard_map/pallas_call | solution.py:481

commit v6 on v5

--- a/solution.py
+++ b/solution.py
@@ -254,10 +254,10 @@
         roots[i] = jnp.concatenate([found[i, top] for top in range(0, ROWS, 16)], axis=0)
 
     land(x_loads[0])
-    start(*x_loads[3:5])
+    start(x_loads[3])
     roots[0] = root(0, 0, ROWS)[0]
     land(gate_load, x_loads[1], *small)
-    start(w_loads[1], x_loads[5])
+    start(w_loads[1], *x_loads[4:])
     bias_row = jnp.concatenate([bias[...], jnp.zeros((1, 112), F32)], axis=1)
     gate([0], roots, squares_of(found, [1], 0, 8, 2))
     collected(1)
@@ -266,11 +266,11 @@
     collected(2)
     gate([2], roots)
 
-    land(w_loads[0], *x_loads[3:5])
+    land(w_loads[0], x_loads[3])
     start(load_q)
     sums_a, sums_b = [None, None], [None, None]
-    project(first_rows, sums_a, range(tiles // 2), squares_of(found, [3, 4], 0, 8), {5: gates})
-    land(w_loads[1], x_loads[5])
+    project(first_rows, sums_a, range(tiles // 2), squares_of(found, [3], 0, 8), {5: gates})
+    land(w_loads[1], *x_loads[4:])
     handed = []
 
     def greet_and_hand():
@@ -289,7 +289,7 @@
             ).start()
 
     project(
-        first_rows, sums_a, range(tiles // 2, tiles), squares_of(found, [5], tiles // 2, 8)
+        first_rows, sums_a, range(tiles // 2, tiles), squares_of(found, [4, 5], tiles // 2, 8)
     )
     for i in range(per_seq, 2 * per_seq):
         collected(i)
@@ -320,7 +320,8 @@
         handed[0].wait()
         scalars()
 
-    between = {2: first_memory, 4: greet_and_hand, 5: lambda: send_memory(0), 9: send_token, 11: arrived_scalars, 13: send_scalars}
+    greet_and_hand()
+    between = {1: first_memory, 3: lambda: send_memory(0), 8: arrived_scalars, 9: send_scalars, 12: send_token}
     project(second_rows, sums_b, range(tiles), None, between)
     value_b, key_b = (total.astype(BF16) for total in sums_b)
     normalizer(1, key_b)
@@ -374,7 +375,7 @@
     lw = sums[:, 0:128] + sums[:, 128:256] + sums[:, 256:384] + pltpu.roll(arrived, 64, 1)
     top = jnp.max(lw, axis=0, keepdims=True)
     scale = jnp.exp(lw - top)
-    stacked = jnp.concatenate([scale, jnp.broadcast_to(top, (8, 128)), jnp.zeros((88, 128), F32)], axis=0)
+    stacked = jnp.concatenate([scale, jnp.broadcast_to(top, (8, 128))], axis=0)
     turned = stacked.T
 
     factor = DH ** (-0.5)

time: 21.9 us -> 21.4 us (0.977)
  Pallas kernels: 21.2 us -> 20.7 us
    pallas_call x1, Pallas kernels: 20.6 us -> 20 us  [shards(): pl.pallas_call(kernel, out_shape=pltpu.VMEM((24, 128), F32), in_specs=[hb...]
where the time goes in v6:
time: 21.4 us; the launch traced here: 21.3 us
  Pallas kernels  20.7 us (97%)
  between operations  0.64 us (3%)
    pallas_call x1, Pallas kernels, shards(): pl.pallas_call(kernel, out_shape=pltpu.VMEM((24, 128), F32), in_specs=[hb...  20 us
    pallas_call x1, Pallas kernels, shards(): pl.pallas_call(unpack, out_shape=out_shape, in_specs=[vmem], out_specs=[v...  0.65 us

profile of v6, /device:TPU:1, one launch (start us, length us, event | category | flops | bytes accessed | tf_op | source)
XLA Modules:
  0.0 21.3 jit_solution(7339607095010024112)
XLA Ops:
  0.6 20.0 %shard_map.111.packed = f32[24,128]{1,0:T(8,128)S(1)} custom-call(bf16[768,4096]{1,0:T(8,128)(2,1)} %bitcast.4, bf16[4096,256]{1,0:T(8,128)(2,1)} %wk_hbm.1, bf16[4096,256]{1,0:T(8,128)(2,1)} %wv_hbm.1, bf16[4096,256]{1,0:T(8,128)(2,1)} %wq_hbm.1, bf16[16,4096]{1,0:T(8,128)(2,1)} %bitcast.5, bf16[16,4096]{1,0:T(8,128)(2,1)} %bitcast.6, f32[1,16]{1,0:T(1,128)} %bitcast.7, ...), custom_call_target="tpu_custom_call" | custom-call | tf_op jit(solution)/shard_map/pallas_call | solution.py:443
  20.7 0.7 %shard_map.112 = (bf16[2,2,4,128]{3,2,1,0:T(4,128)(2,1)}, f32[2,2,4]{2,1,0:T(2,128)}, f32[2,2]{1,0:T(2,128)}, bf16[2,2,4]{2,1,0:T(2,128)(2,1)}) custom-call(f32[24,128]{1,0:T(8,128)S(1)} %shard_map.111.packed), custom_call_target="tpu_custom_call" | custom-call | tf_op jit(solution)/shard_map/pallas_call | solution.py:482

commit v7 on v6

--- a/solution.py
+++ b/solution.py
@@ -414,7 +414,7 @@
         at = pl.ds(pl.multiple_of(8 * order[s], 8), 8)
         table[at, :] = jnp.where(lane8 == 0, own_normal, jnp.where(lane8 == 1, top_col, read))
         packed_out[at, :] = merged
-    packed_out[16:24] = jnp.concatenate([table[...], jnp.zeros((112, 128), F32)], axis=0).T[0:8]
+    packed_out[16:24, 0:16] = table[...].T[0:8]
 
 
 def unpack(packed, mat_out, nrm_out, top_out, read_out):

time: 21.4 us -> 21.4 us (level)
  no operation moved by 1% of the time
where the time goes in v7:
time: 21.4 us; the launch traced here: 21.3 us
  Pallas kernels  20.7 us (97%)
  between operations  0.64 us (3%)
    pallas_call x1, Pallas kernels, shards(): pl.pallas_call(kernel, out_shape=pltpu.VMEM((24, 128), F32), in_specs=[hb...  20 us
    pallas_call x1, Pallas kernels, shards(): pl.pallas_call(unpack, out_shape=out_shape, in_specs=[vmem], out_specs=[v...  0.65 us

profile of v7, /device:TPU:1, one launch (start us, length us, event | category | flops | bytes accessed | tf_op | source)
XLA Modules:
  0.0 21.3 jit_solution(12527073697725741630)
XLA Ops:
  0.6 20.0 %shard_map.111.packed = f32[24,128]{1,0:T(8,128)S(1)} custom-call(bf16[768,4096]{1,0:T(8,128)(2,1)} %bitcast.4, bf16[4096,256]{1,0:T(8,128)(2,1)} %wk_hbm.1, bf16[4096,256]{1,0:T(8,128)(2,1)} %wv_hbm.1, bf16[4096,256]{1,0:T(8,128)(2,1)} %wq_hbm.1, bf16[16,4096]{1,0:T(8,128)(2,1)} %bitcast.5, bf16[16,4096]{1,0:T(8,128)(2,1)} %bitcast.6, f32[1,16]{1,0:T(1,128)} %bitcast.7, ...), custom_call_target="tpu_custom_call" | custom-call | tf_op jit(solution)/shard_map/pallas_call | solution.py:443
  20.7 0.7 %shard_map.112 = (bf16[2,2,4,128]{3,2,1,0:T(4,128)(2,1)}, f32[2,2,4]{2,1,0:T(2,128)}, f32[2,2]{1,0:T(2,128)}, bf16[2,2,4]{2,1,0:T(2,128)(2,1)}) custom-call(f32[24,128]{1,0:T(8,128)S(1)} %shard_map.111.packed), custom_call_target="tpu_custom_call" | custom-call | tf_op jit(solution)/shard_map/pallas_call | solution.py:482
